TPU v7x, 32 devices: a whole 2x2x4 slice. The times are simulated.
32 devices in a mesh: gr: 2 (over core), fs: 8 (over z, y), tp: 2 (over x).
Axes of the slice: x: 2, y: 2, z: 4, core: 2. Of those that a mesh axis runs over, the one named last changes fastest.
Arguments:
- tokens: bfloat16 [3072, 2048], P(('gr', 'fs')), may hold values from -6 to 6
- routes: int32 [3072, 8], P(('gr', 'fs')), may hold values from 0 to 15, all different within a row; in each aligned block of 192 rows (0 to 191, 192 to 383, ...) at most 144 rows name the same one
- route_weight: float32 [3072, 8], P(('gr', 'fs')), may hold values from 0.05 to 0.6
- norm_gain: float32 [2048], replicated, may hold values from 0.1 to 1.9
- gate_experts: float32 [2, 8, 512, 2048], P('gr', None, 'fs', 'tp'), may hold values from -0.125 to 0.125
- up_experts: float32 [2, 8, 512, 2048], P('gr', None, 'fs', 'tp'), may hold values from -0.125 to 0.125
- down_experts: float32 [2, 8, 512, 2048], P('gr', None, 'fs', 'tp'), may hold values from -0.25 to 0.25
- gate_shared: float32 [2048, 512], P('fs', 'tp'), may hold values from -0.125 to 0.125
- up_shared: float32 [2048, 512], P('fs', 'tp'), may hold values from -0.125 to 0.125
- down_shared: float32 [512, 2048], P('fs', 'tp'), may hold values from -0.25 to 0.25
Outputs:
- mixed: bfloat16 [3072, 2048], P(('gr', 'fs'), 'tp')
- gate_served: bfloat16 [2, 8, 512, 2048], P(None, 'fs', 'tp')
- up_served: bfloat16 [2, 8, 512, 2048], P(None, 'fs', 'tp')
- down_served: bfloat16 [2, 8, 512, 2048], P(None, 'fs', None, 'tp')
- gate_shared_served: bfloat16 [2048, 512], P(None, 'tp')
- up_shared_served: bfloat16 [2048, 512], P(None, 'tp')
- down_shared_served: bfloat16 [512, 2048], P(None, 'tp')
Inputs may be any that keep to these rules, and one draw needn't show every extreme that they name: `routes`: each row names 8 different experts; within the 192 rows of one device no expert is named by more than 144 rows, and some expert reaches 144.
All inputs are finite; a program needn't handle non-finite values.
Results may differ from a plain program's by a relative error of at most 0.0084.
Values may be sent and summed in bfloat16 or wider, within the bound.
A program may use at most 128 MiB of HBM per device.

v0:
```python
import jax
import jax.numpy as jnp
from jax import lax
from jax.sharding import PartitionSpec as P

EXP_HALF = 1


EPS = 1e-06


def on_device(
    tokens,
    routes,
    route_weight,
    norm_gain,
    gate_experts,
    up_experts,
    down_experts,
    gate_shared,
    up_shared,
    down_shared,
):
    bf = jnp.bfloat16
    f32 = jnp.float32
    n_fs = lax.axis_size("fs")
    n_gr = lax.axis_size("gr")
    n_tp = lax.axis_size("tp")
    fs_index = lax.axis_index("fs")
    cols_here = gate_experts.shape[3]
    gain_cols = lax.dynamic_slice_in_dim(norm_gain, lax.axis_index("tp") * cols_here, cols_here, 0)
    gate_local = (gate_experts * gain_cols[None, None, None, :]).astype(bf)
    up_local = (up_experts * gain_cols[None, None, None, :]).astype(bf)
    down_local = down_experts.astype(bf)
    shared_here = gate_shared.shape[0]
    gain_shared = lax.dynamic_slice_in_dim(norm_gain, fs_index * shared_here, shared_here, 0)
    gate_sh_local = (gate_shared * gain_shared[:, None]).astype(bf)
    up_sh_local = (up_shared * gain_shared[:, None]).astype(bf)
    down_sh_local = down_shared.astype(bf)
    halves = (
        lax.all_gather(gate_local, "gr", axis=0, tiled=True),
        lax.all_gather(up_local, "gr", axis=0, tiled=True),
        lax.all_gather(down_local, "gr", axis=0, tiled=True),
    )
    gate_cols, up_cols, down_w = (
        lax.all_to_all(halves[0], "fs", split_axis=1, concat_axis=2, tiled=True),
        lax.all_to_all(halves[1], "fs", split_axis=1, concat_axis=2, tiled=True),
        lax.all_to_all(halves[2], "fs", split_axis=1, concat_axis=2, tiled=True),
    )
    gate_w, up_w = (
        lax.all_to_all(gate_cols, "tp", split_axis=2, concat_axis=3, tiled=True),
        lax.all_to_all(up_cols, "tp", split_axis=2, concat_axis=3, tiled=True),
    )
    gate_sw, up_sw, down_sw = (
        lax.all_gather(gate_sh_local, "fs", axis=0, tiled=True),
        lax.all_gather(up_sh_local, "fs", axis=0, tiled=True),
        lax.all_gather(down_sh_local, "fs", axis=0, tiled=True),
    )
    values = tokens.astype(f32)
    normed = (values * lax.rsqrt(jnp.mean(values * values, axis=-1, keepdims=True) + EPS)).astype(
        bf
    )
    tok_count, top = routes.shape
    width = tokens.shape[1]
    per_group = gate_experts.shape[1]
    count = per_group * n_gr
    capacity = (3 * tok_count * top + 2 * count - 1) // (2 * count)
    flat_e = routes.reshape(-1)
    onehot = (flat_e[:, None] == jnp.arange(count, dtype=jnp.int32)[None, :]).astype(jnp.int32)
    ranks = jnp.sum(jnp.cumsum(onehot, axis=0) * onehot, axis=1) - 1
    group_of = flat_e // per_group
    within = flat_e % per_group
    target = within // EXP_HALF
    local_k = within % EXP_HALF
    slot = ((target * n_gr + group_of) * EXP_HALF + local_k) * capacity + ranks
    total_slots = n_fs * n_gr * EXP_HALF * capacity
    repeated = jnp.repeat(normed, top, axis=0)
    send = jnp.zeros((total_slots, width), bf).at[slot].set(repeated)
    send = send.reshape(n_fs, n_gr, EXP_HALF, capacity, width)
    cols = width // n_tp
    send = lax.dynamic_slice_in_dim(send, lax.axis_index("tp") * cols, cols, 4)
    received = lax.all_to_all(send, "fs", split_axis=0, concat_axis=0, tiled=True)
    received = lax.all_gather(received, "tp", axis=4, tiled=True)
    gate = jnp.einsum("sgkcd,gkfd->sgkcf", received, gate_w, preferred_element_type=f32)
    upper = jnp.einsum("sgkcd,gkfd->sgkcf", received, up_w, preferred_element_type=f32)
    hidden = (jax.nn.silu(gate) * upper).astype(bf)
    full_hidden = lax.all_gather(hidden, "tp", axis=4, tiled=True)
    result = jnp.einsum(
        "sgkcf,gkfe->sgkce", full_hidden, down_w, preferred_element_type=f32
    ).astype(bf)
    returned = lax.all_to_all(result, "fs", split_axis=0, concat_axis=0, tiled=True)
    picked = returned.reshape(total_slots, cols)[slot].reshape(tok_count, top, cols)
    routed = jnp.einsum("tkc,tk->tc", picked.astype(f32), route_weight)
    shared_gate = jnp.dot(normed, gate_sw, preferred_element_type=f32)
    shared_up = jnp.dot(normed, up_sw, preferred_element_type=f32)
    shared_hidden = (jax.nn.silu(shared_gate) * shared_up).astype(bf)
    shared_full = lax.all_gather(shared_hidden, "tp", axis=1, tiled=True)
    shared = jnp.dot(shared_full, down_sw, preferred_element_type=f32)
    mixed = (routed + shared).astype(bf)
    return (mixed, gate_w, up_w, down_w, gate_sw, up_sw, down_sw)


def solution(mesh):
    return jax.shard_map(
        on_device,
        mesh=mesh,
        in_specs=(
            P(("gr", "fs"), None),
            P(("gr", "fs"), None),
            P(("gr", "fs"), None),
            P(),
            P("gr", None, "fs", "tp"),
            P("gr", None, "fs", "tp"),
            P("gr", None, "fs", "tp"),
            P("fs", "tp"),
            P("fs", "tp"),
            P("fs", "tp"),
        ),
        out_specs=(
            P(("gr", "fs"), "tp"),
            P(None, "fs", "tp", None),
            P(None, "fs", "tp", None),
            P(None, "fs", None, "tp"),
            P(None, "tp"),
            P(None, "tp"),
            P(None, "tp"),
        ),
        check_vma=False,
    )
```

profile of v0, /device:TPU:0, one launch (start us, length us, event | category | flops | bytes accessed | tf_op | source)
XLA Modules:
  0.0 651.1 jit_solution(783318843968911715)
XLA Ops:
  9.2 4.5 reduce-window.6
  16.2 14.7 %scatter_custom_fusion = bf16[2304,2048]{1,0:T(8,128)(2,1)} fusion(s32[1536]{0:T(1024)S(1)} %fusion.28, bf16[]{:T(256)} %constant.72.clone.1, bf16[192,2048]{1,0:T(8,128)(2,1)S(1)} %fusion.22), kind=kCustom, calls=%fused_computation.6 | custom fusion | bytes 10223618 | tf_op jit(solution)/shard_map/scatter | solution.py:78
  30.9 5.3 dynamic-slice_bitcast_fusion
  36.2 7.4 %all-to-all-start.2 = ((bf16[8,2,1,144,1024]{4,3,1,2,0:T(8,128)(2,1)}), bf16[8,2,1,144,1024]{4,3,1,2,0:T(8,128)(2,1)}, u32[]{:S(2)}, u32[]{:S(2)}) async-start(bf16[8,2,1,144,1024]{4,3,1,2,0:T(8,128)(2,1)} %dynamic-slice_bitcast_fusion), calls=%async_computation.2 | async-start | bytes 9437184 | tf_op jit(solution)/shard_map/all_to_all | solution.py:82
  43.7 3.5 multiply_convert_fusion.1
  49.9 9.4 %all-gather.13.cloned.1.call-done = bf16[2,8,64,1024]{3,2,1,0:T(8,128)(2,1)} async-done(((bf16[1,8,64,1024]{3,2,1,0:T(8,128)(2,1)}), bf16[2,8,64,1024]{3,2,1,0:T(8,128)(2,1)}) %all-gather.13.cloned.1.call-update) | async-done | bytes 2097168 | tf_op jit(solution)/shard_map/all_gather | solution.py:42
  59.3 3.1 copy.63
  62.4 85.7 %all-to-all-done.2 = bf16[8,2,1,144,1024]{4,3,1,2,0:T(8,128)(2,1)} async-done(((bf16[8,2,1,144,1024]{4,3,1,2,0:T(8,128)(2,1)}), bf16[8,2,1,144,1024]{4,3,1,2,0:T(8,128)(2,1)}, u32[]{:S(2)}, u32[]{:S(2)}) %all-to-all-start.2) | async-done | bytes 4718624 | tf_op jit(solution)/shard_map/all_to_all | solution.py:82
  148.2 3.6 all-to-all-start.3
  152.0 5.3 copy.62
  157.3 3.1 copy.53
  160.5 39.7 %all-to-all-done.3 = bf16[2,8,64,1024]{3,2,0,1:T(8,128)(2,1)S(1)} async-done(((bf16[2,8,64,1024]{3,2,0,1:T(8,128)(2,1)}), bf16[2,8,64,1024]{3,2,0,1:T(8,128)(2,1)S(1)}, u32[]{:S(2)}, u32[]{:S(2)}) %all-to-all-start.3) | async-done | bytes 2097184 | tf_op jit(solution)/shard_map/all_to_all | solution.py:47
  200.2 4.4 all-to-all-start
  204.8 3.5 copy.65
  208.2 44.2 %all-to-all-done = bf16[2,8,64,1024]{3,2,0,1:T(8,128)(2,1)} async-done(((bf16[2,8,64,1024]{3,2,0,1:T(8,128)(2,1)}), bf16[2,8,64,1024]{3,2,0,1:T(8,128)(2,1)}, u32[]{:S(2)}, u32[]{:S(2)}) %all-to-all-start) | async-done | bytes 2097184 | tf_op jit(solution)/shard_map/all_to_all | solution.py:46
  252.4 3.8 all-to-all-start.4
  256.2 1.8 copy.54
  257.9 3.5 copy.55
  261.4 37.6 %all-to-all-done.4 = bf16[2,1,512,1024]{3,0,1,2:T(2,128)(2,1)S(1)} async-done(((bf16[2,1,512,1024]{3,0,1,2:T(2,128)(2,1)}), bf16[2,1,512,1024]{3,0,1,2:T(2,128)(2,1)S(1)}, u32[]{:S(2)}, u32[]{:S(2)}) %all-to-all-start.4) | async-done | bytes 2097184 | tf_op jit(solution)/shard_map/all_to_all | solution.py:52
  299.0 4.8 all-to-all-start.1
  303.9 3.1 copy.68
  307.0 2.2 copy.66
  309.3 3.5 copy.67
  312.7 4.5 reshape.245
  317.2 11.3 %all-to-all-done.1 = bf16[2,1,512,1024]{3,0,1,2:T(2,128)(2,1)} async-done(((bf16[2,1,512,1024]{3,0,1,2:T(2,128)(2,1)}), bf16[2,1,512,1024]{3,0,1,2:T(2,128)(2,1)}, u32[]{:S(2)}, u32[]{:S(2)}) %all-to-all-start.1) | async-done | bytes 2097184 | tf_op jit(solution)/shard_map/all_to_all | solution.py:51
  328.5 6.1 all-to-all-start.5
  334.8 2.2 copy.56
  338.4 3.5 copy.57
  341.8 4.5 reshape.244
  346.3 6.0 fusion
  354.0 4.1 fusion.10
  358.1 24.0 %all-to-all-done.5 = bf16[2,8,64,1024]{3,2,0,1:T(8,128)(2,1)} async-done(((bf16[2,8,64,1024]{3,2,0,1:T(8,128)(2,1)}), bf16[2,8,64,1024]{3,2,0,1:T(8,128)(2,1)}, u32[]{:S(2)}, u32[]{:S(2)}) %all-to-all-start.5) | async-done | bytes 2097184 | tf_op jit(solution)/shard_map/all_to_all | solution.py:48
  382.1 3.1 copy.69
  385.2 9.5 %all-gather.15.cloned.1.call-done = bf16[8,2,1,144,512]{4,3,0,1,2:T(8,128)(2,1)} async-done(((bf16[8,2,1,144,256]{4,3,0,1,2:T(8,128)(2,1)}), bf16[8,2,1,144,512]{4,3,0,1,2:T(8,128)(2,1)}) %all-gather.15.cloned.1.call-update) | async-done | bytes 2359312 | tf_op jit(solution)/shard_map/all_gather | solution.py:87
  394.7 4.9 convert_bitcast_fusion
  399.7 2.7 copy.70
  402.4 5.7 all-to-all-start.6
  408.2 1.8 multiply_convert_fusion.3
  411.5 114.1 %all-gather.19.cloned.1.call-done = bf16[2048,256]{1,0:T(8,128)(2,1)} async-done(((bf16[256,256]{1,0:T(8,128)(2,1)}), bf16[2048,256]{1,0:T(8,128)(2,1)}) %all-gather.19.cloned.1.call-update) | async-done | bytes 1048592 | tf_op jit(solution)/shard_map/all_gather | solution.py:55
  525.6 39.1 %all-gather.21.cloned.1.call-done = bf16[2048,256]{1,0:T(8,128)(2,1)} async-done(((bf16[256,256]{1,0:T(8,128)(2,1)}), bf16[2048,256]{1,0:T(8,128)(2,1)}) %all-gather.21.cloned.1.call-update) | async-done | bytes 1048592 | tf_op jit(solution)/shard_map/all_gather | solution.py:56
  564.7 41.5 %all-gather.23.cloned.1.call-done = bf16[512,1024]{1,0:T(8,128)(2,1)} async-done(((bf16[64,1024]{1,0:T(8,128)(2,1)}), bf16[512,1024]{1,0:T(8,128)(2,1)}) %all-gather.23.cloned.1.call-update) | async-done | bytes 1048592 | tf_op jit(solution)/shard_map/all_gather | solution.py:57
  607.9 1.6 fusion.24
  609.5 5.5 all_gather.34
  615.0 3.9 copy.71
  618.9 2.6 copy.72
  621.5 4.1 copy.74
  625.6 2.4 copy.75
  628.0 10.0 %gather_fusion = bf16[1536,1024]{1,0:T(8,128)(2,1)S(1)} fusion(bf16[2304,1024]{1,0:T(8,128)(2,1)} %bitcast.25, s32[2048]{0:T(1024)S(1)} %pad_clamp_fusion), kind=kCustom, calls=%fused_computation | custom fusion | bytes 6297600 | tf_op jit(solution)/shard_map/gather | solution.py:92
  (78 shorter events, 18.5 us)
Async XLA Ops:
  8.0 8.0 %copy-start.5 = (bf16[192,2048]{1,0:T(8,128)(2,1)S(1)}, bf16[192,2048]{1,0:T(8,128)(2,1)}, u32[]{:S(2)}) copy-start(bf16[192,2048]{1,0:T(8,128)(2,1)} %param.10) | copy-start | bytes 2359300
  36.2 7.5 %copy-start.8 = (f32[1,8,64,1024]{3,2,1,0:T(8,128)S(1)}, f32[1,8,64,1024]{3,2,1,0:T(8,128)}, u32[]{:S(2)}) copy-start(f32[1,8,64,1024]{3,2,1,0:T(8,128)} %param.14) | copy-start | bytes 6291460
  36.2 7.5 %dynamic-slice-start = ((f32[2048]{0:T(1024)}, s32[]{:T(128)}), f32[1024]{0:T(1024)S(1)}, s32[]{:S(2)}) async-start(f32[2048]{0:T(1024)} %param.13, s32[]{:T(128)} %select_n.52), calls=%async_computation.15 | async-start | bytes 8704 | tf_op jit(solution)/shard_map/dynamic_slice | solution.py:31
  36.2 112.0 %all-to-all-start.2 = ((bf16[8,2,1,144,1024]{4,3,1,2,0:T(8,128)(2,1)}), bf16[8,2,1,144,1024]{4,3,1,2,0:T(8,128)(2,1)}, u32[]{:S(2)}, u32[]{:S(2)}) async-start(bf16[8,2,1,144,1024]{4,3,1,2,0:T(8,128)(2,1)} %dynamic-slice_bitcast_fusion), calls=%async_computation.2 | async-start | bytes 9437184 | tf_op jit(solution)/shard_map/all_to_all | solution.py:82
  43.6 15.7 %all-gather.13.cloned.1.call-start = ((), (), s32[]{:S(2)}) async-start(), calls=%async_computation.9 | async-start | bytes 3145728 | tf_op jit(solution)/shard_map/all_gather | solution.py:42
  47.2 1.6 copy-start.6
  47.2 110.1 %all-gather.9.cloned.1.call-start = ((), (), s32[]{:S(2)}) async-start(), calls=%async_computation.7 | async-start | bytes 3145728 | tf_op jit(solution)/shard_map/all_gather | solution.py:41
  48.0 255.9 %all-gather.17.cloned.1.call-start = ((), (), s32[]{:S(2)}) async-start(), calls=%async_computation.11 | async-start | bytes 3145728 | tf_op jit(solution)/shard_map/all_gather | solution.py:43
  148.2 52.1 %all-to-all-start.3 = ((bf16[2,8,64,1024]{3,2,0,1:T(8,128)(2,1)}), bf16[2,8,64,1024]{3,2,0,1:T(8,128)(2,1)S(1)}, u32[]{:S(2)}, u32[]{:S(2)}) async-start(bf16[2,8,64,1024]{3,2,0,1:T(8,128)(2,1)} %copy.63), calls=%async_computation.3 | async-start | bytes 4194304 | tf_op jit(solution)/shard_map/all_to_all | solution.py:47
  151.8 194.5 %all-gather.11.cloned.1.call-start = ((), (), s32[]{:S(2)}) async-start(), calls=%async_computation.8 | async-start | bytes 14155776 | tf_op jit(solution)/shard_map/all_gather | solution.py:83
  200.2 52.2 %all-to-all-start = ((bf16[2,8,64,1024]{3,2,0,1:T(8,128)(2,1)}), bf16[2,8,64,1024]{3,2,0,1:T(8,128)(2,1)}, u32[]{:S(2)}, u32[]{:S(2)}) async-start(bf16[2,8,64,1024]{3,2,0,1:T(8,128)(2,1)} %copy.53), calls=%async_computation | async-start | bytes 4194304 | tf_op jit(solution)/shard_map/all_to_all | solution.py:46
  252.4 46.6 %all-to-all-start.4 = ((bf16[2,1,512,1024]{3,0,1,2:T(2,128)(2,1)}), bf16[2,1,512,1024]{3,0,1,2:T(2,128)(2,1)S(1)}, u32[]{:S(2)}, u32[]{:S(2)}) async-start(bf16[2,1,512,1024]{3,0,1,2:T(2,128)(2,1)} %copy.65), calls=%async_computation.4 | async-start | bytes 4194304 | tf_op jit(solution)/shard_map/all_to_all | solution.py:52
  299.0 4.9 copy-start.1
  299.0 29.5 %all-to-all-start.1 = ((bf16[2,1,512,1024]{3,0,1,2:T(2,128)(2,1)}), bf16[2,1,512,1024]{3,0,1,2:T(2,128)(2,1)}, u32[]{:S(2)}, u32[]{:S(2)}) async-start(bf16[2,1,512,1024]{3,0,1,2:T(2,128)(2,1)} %copy.55), calls=%async_computation.1 | async-start | bytes 4194304 | tf_op jit(solution)/shard_map/all_to_all | solution.py:51
  328.5 53.6 %all-to-all-start.5 = ((bf16[2,8,64,1024]{3,2,0,1:T(8,128)(2,1)}), bf16[2,8,64,1024]{3,2,0,1:T(8,128)(2,1)}, u32[]{:S(2)}, u32[]{:S(2)}) async-start(bf16[2,8,64,1024]{3,2,0,1:T(8,128)(2,1)} %copy.68), calls=%async_computation.5 | async-start | bytes 4194304 | tf_op jit(solution)/shard_map/all_to_all | solution.py:48
  334.6 60.1 %all-gather.15.cloned.1.call-start = ((), (), s32[]{:S(2)}) async-start(), calls=%async_computation.10 | async-start | bytes 3538944 | tf_op jit(solution)/shard_map/all_gather | solution.py:87
  337.0 1.3 copy-start
  346.3 6.0 copy-start.7
  346.3 7.6 %copy-start.14 = (bf16[8,2,1,144,2048]{4,3,0,1,2:T(8,128)(2,1)S(1)}, bf16[8,2,1,144,2048]{4,3,0,1,2:T(8,128)(2,1)}, u32[]{:S(2)}) copy-start(bf16[8,2,1,144,2048]{4,3,0,1,2:T(8,128)(2,1)} %all-gather.11.cloned.1.call-done) | copy-start | bytes 28311556
  402.4 5.7 copy-start.12
  402.4 5.8 copy-start.11
  402.4 8.2 %copy-start.10 = (f32[64,1024]{1,0:T(8,128)S(1)}, f32[64,1024]{1,0:T(8,128)}, u32[]{:S(2)}) copy-start(f32[64,1024]{1,0:T(8,128)} %param.19) | copy-start | bytes 786436
  402.4 8.9 %copy-start.13 = (f32[192,8]{0,1:T(8,128)S(1)}, f32[192,8]{0,1:T(8,128)}, u32[]{:S(2)}) copy-start(f32[192,8]{0,1:T(8,128)} %param.12) | copy-start | bytes 18436
  402.4 225.6 %all-to-all-start.6 = ((bf16[8,2,1,144,1024]{4,3,1,2,0:T(8,128)(2,1)}), bf16[8,2,1,144,1024]{4,3,1,2,0:T(8,128)(2,1)}, u32[]{:S(2)}, u32[]{:S(2)}) async-start(bf16[8,2,1,144,1024]{4,3,1,2,0:T(8,128)(2,1)} %copy.70), calls=%async_computation.6 | async-start | bytes 9437184 | tf_op jit(solution)/shard_map/all_to_all | solution.py:91
  408.1 117.5 %all-gather.19.cloned.1.call-start = ((), (), s32[]{:S(2)}) async-start(), calls=%async_computation.12 | async-start | bytes 1179648 | tf_op jit(solution)/shard_map/all_gather | solution.py:55
  410.0 154.7 %all-gather.21.cloned.1.call-start = ((), (), s32[]{:S(2)}) async-start(), calls=%async_computation.13 | async-start | bytes 1179648 | tf_op jit(solution)/shard_map/all_gather | solution.py:56
  410.6 195.7 %all-gather.23.cloned.1.call-start = ((), (), s32[]{:S(2)}) async-start(), calls=%async_computation.14 | async-start | bytes 1179648 | tf_op jit(solution)/shard_map/all_gather | solution.py:57
  621.5 4.1 copy-start.2
  638.0 1.2 copy-start.3
  638.0 2.4 copy-start.4
  639.3 2.1 copy-start.9
Sparse Core Ops, SparseCore 0:
  47.3 11.9 all-gather.12
  61.4 11.7 all-gather.8
  75.3 11.7 all-gather.16
  157.4 137.9 all-gather.10
  358.2 36.4 all-gather.14
Sparse Core Ops, SparseCore 1:
  411.2 114.3 all-gather.18
  528.2 36.5 all-gather.20
  567.3 38.9 all-gather.22
where the time goes:
time: 660 us; the launch traced here: 651 us
  waiting for transfers between devices  457 us (69%)
  local copies, waits for them, and re-layouts  101 us (15%)
  starting transfers between devices  36.5 us (6%)
  matrix products  20.4 us (3%)
  between operations  16.2 us (2%)
  other arithmetic  13.6 us (2%)
    all_gather x1, waiting for transfers between devices, on_device(): lax.all_gather(gate_sh_local, 'fs', axis=0, tiled=True)  114 us
    all_to_all x1, waiting for transfers between devices, on_device(): lax.all_to_all(send, 'fs', split_axis=0, concat_axis=0, tiled=True)  85.7 us
    all_to_all x1, waiting for transfers between devices, on_device(): lax.all_to_all(halves[0], 'fs', split_axis=1, concat_axis=2, tiled=True)  44.2 us
    all_gather x1, waiting for transfers between devices, on_device(): lax.all_gather(down_sh_local, 'fs', axis=0, tiled=True)  41.5 us
    all_to_all x1, waiting for transfers between devices, on_device(): lax.all_to_all(halves[1], 'fs', split_axis=1, concat_axis=2, tiled=True)  39.7 us
    all_gather x1, waiting for transfers between devices, on_device(): lax.all_gather(up_sh_local, 'fs', axis=0, tiled=True)  39.1 us
    all_to_all x1, waiting for transfers between devices, on_device(): lax.all_to_all(up_cols, 'tp', split_axis=2, concat_axis=3, tiled=True)  37.6 us
    all_to_all x1, waiting for transfers between devices, on_device(): lax.all_to_all(halves[2], 'fs', split_axis=1, concat_axis=2, tiled=True)  24 us
  transfers between devices with their start and end apart: 15, of which 11 were waited for; matrix products, arithmetic and copies ran while one was open for 12% of the time, Pallas kernels for 0%

commit v1 on v0

v1 whole, which is shorter than its diff:
```python
import jax
import jax.numpy as jnp
from jax import lax
from jax.experimental import pallas as pl
from jax.experimental.pallas import tpu as pltpu
from jax.sharding import PartitionSpec as P

EPS = 1e-06
MESH = pl.DeviceIdType.MESH


def exchange_kernel(dims, g_loc, u_loc, d_loc, g_out, u_out, d_out, send, recv, d_send, d_recv,
                    own, f_send, f_recv, fd_send, fd_recv):
    n_gr, n_fs, n_tp = dims
    gr, fs, tp = lax.axis_index("gr"), lax.axis_index("fs"), lax.axis_index("tp")
    held = g_loc.shape[0] // n_fs
    rows, cols = g_loc.shape[1], g_loc.shape[2]
    per = g_out.shape[2] // rows
    barrier = pltpu.get_barrier_semaphore()

    def greet(i, carry):
        f, t = i // n_tp, i % n_tp

        @pl.when((f != fs) | (t != tp))
        def _():
            pl.semaphore_signal(barrier, inc=1, device_id=(gr, f, t), device_id_type=MESH)
        return carry

    lax.fori_loop(0, n_fs * n_tp, greet, 0)
    for p in range(1, n_gr):
        pl.semaphore_signal(
            barrier, inc=1, device_id=((gr + p) % n_gr, fs, tp), device_id_type=MESH
        )
    pl.semaphore_wait(barrier, n_fs * n_tp - 1 + n_gr - 1)

    to_tp = fs // per
    mine = pl.multiple_of(tp * cols, cols)

    def wide(loc, out, m, d):
        k = (fs + d) % n_fs
        return pltpu.make_async_remote_copy(
            src_ref=loc.at[pl.ds(k * held, held)],
            dst_ref=out.at[gr, :, pl.ds(pl.multiple_of((fs % per) * rows, rows), rows), pl.ds(mine, cols)],
            send_sem=send.at[m, d],
            recv_sem=recv.at[m, fs % per, tp],
            device_id=(gr, k, to_tp),
            device_id_type=MESH,
        )

    def wide_own(loc, out, m):
        return pltpu.make_async_copy(
            loc.at[pl.ds(fs * held, held)],
            out.at[gr, :, pl.ds(pl.multiple_of((fs % per) * rows, rows), rows), pl.ds(mine, cols)],
            own.at[m],
        )

    def tall(d):
        k = (fs + d) % n_fs
        return pltpu.make_async_remote_copy(
            src_ref=d_loc.at[pl.ds(k * held, held)],
            dst_ref=d_out.at[gr, :, pl.ds(pl.multiple_of(fs * rows, rows), rows), :],
            send_sem=d_send.at[d],
            recv_sem=d_recv.at[fs],
            device_id=(gr, k, tp),
            device_id_type=MESH,
        )

    tall_own = pltpu.make_async_copy(
        d_loc.at[pl.ds(fs * held, held)],
        d_out.at[gr, :, pl.ds(pl.multiple_of(fs * rows, rows), rows), :],
        own.at[2],
    )
    pairs = ((g_loc, g_out, 0), (u_loc, u_out, 1))
    order = [d for d in range(1, n_fs)] + [0]
    for loc, out, m in pairs:
        for d in order:
            if d:
                wide(loc, out, m, d).start()
            else:
                @pl.when(to_tp == tp)
                def _():
                    wide_own(loc, out, m).start()

                @pl.when(to_tp != tp)
                def _():
                    wide(loc, out, m, 0).start()
    for d in range(1, n_fs):
        tall(d).start()
    tall_own.start()

    def forward(block, s_sem, r_sem, p):
        return pltpu.make_async_remote_copy(
            src_ref=block, dst_ref=block, send_sem=s_sem, recv_sem=r_sem,
            device_id=((gr + p) % n_gr, fs, tp), device_id_type=MESH,
        )

    def landed(block, r_sem):
        pltpu.make_async_remote_copy(
            src_ref=block, dst_ref=block, send_sem=r_sem, recv_sem=r_sem,
            device_id=((gr + 1) % n_gr, fs, tp), device_id_type=MESH,
        ).wait_recv()

    def wide_block(out, g, j, t):
        return out.at[g, :, pl.ds(j * rows, rows), pl.ds(t * cols, cols)]

    for loc, out, m in pairs:
        for j in range(per):
            for t in range(n_tp):
                here = (tp * per + j == fs) & (tp == t)

                @pl.when(here)
                def _():
                    wide_own(loc, out, m).wait()

                @pl.when(jnp.logical_not(here))
                def _():
                    landed(wide_block(out, gr, j, t), recv.at[m, j, t])
                for p in range(1, n_gr):
                    forward(wide_block(out, gr, j, t), f_send.at[m, j, t, p - 1],
                            f_recv.at[m, j, t, p - 1], p).start()

    def tall_block(g, s):
        return d_out.at[g, :, pl.ds(s * rows, rows), :]

    for s in range(n_fs):
        @pl.when(s == fs)
        def _():
            tall_own.wait()

        @pl.when(s != fs)
        def _():
            landed(tall_block(gr, s), d_recv.at[s])
        for p in range(1, n_gr):
            forward(tall_block(gr, s), fd_send.at[s, p - 1], fd_recv.at[s, p - 1], p).start()

    for loc, out, m in pairs:
        for d in order:
            if d:
                wide(loc, out, m, d).wait_send()
            else:
                @pl.when(to_tp != tp)
                def _():
                    wide(loc, out, m, 0).wait_send()
        for j in range(per):
            for t in range(n_tp):
                for p in range(1, n_gr):
                    forward(wide_block(out, gr, j, t), f_send.at[m, j, t, p - 1],
                            f_recv.at[m, j, t, p - 1], p).wait_send()
                    landed(wide_block(out, (gr + n_gr - p) % n_gr, j, t), f_recv.at[m, j, t, p - 1])
    for d in range(1, n_fs):
        tall(d).wait_send()
    for s in range(n_fs):
        for p in range(1, n_gr):
            forward(tall_block(gr, s), fd_send.at[s, p - 1], fd_recv.at[s, p - 1], p).wait_send()
            landed(tall_block((gr + n_gr - p) % n_gr, s), fd_recv.at[s, p - 1])


def exchange(dims, g_loc, u_loc, d_loc):
    n_gr, n_fs, n_tp = dims
    count, rows, cols = g_loc.shape
    held = count // n_fs
    units = n_fs * rows
    bf = jnp.bfloat16
    per = units // n_tp // rows
    dma = pltpu.SemaphoreType.DMA
    wide = jax.ShapeDtypeStruct((n_gr, held, units // n_tp, n_tp * cols), bf)
    tall = jax.ShapeDtypeStruct((n_gr, held, units, cols), bf)
    sent = 3 * count * rows * cols * 2

    def body(*refs):
        exchange_kernel(dims, *refs)

    return pl.pallas_call(
        body,
        out_shape=(wide, wide, tall),
        in_specs=[pl.BlockSpec(memory_space=pl.ANY)] * 3,
        out_specs=[pl.BlockSpec(memory_space=pl.ANY)] * 3,
        scratch_shapes=[
            dma((2, n_fs)), dma((2, per, n_tp)), dma((n_fs,)), dma((n_fs,)), dma((3,)),
            dma((2, per, n_tp, n_gr - 1)), dma((2, per, n_tp, n_gr - 1)),
            dma((n_fs, n_gr - 1)), dma((n_fs, n_gr - 1)),
        ],
        compiler_params=pltpu.CompilerParams(collective_id=1, has_side_effects=True),
        cost_estimate=pl.CostEstimate(flops=0, bytes_accessed=100 * sent, transcendentals=0),
    )(g_loc, u_loc, d_loc)


def on_device(tokens, routes, route_weight, norm_gain, gate_experts, up_experts, down_experts,
              gate_shared, up_shared, down_shared):
    bf = jnp.bfloat16
    f32 = jnp.float32
    dims = (lax.axis_size("gr"), lax.axis_size("fs"), lax.axis_size("tp"))
    n_gr, n_fs, n_tp = dims
    fs_index = lax.axis_index("fs")
    tp_index = lax.axis_index("tp")
    cols = gate_experts.shape[3]
    per_group = gate_experts.shape[1]
    count = per_group * n_gr
    held = per_group // n_fs
    tok_count, top = routes.shape
    width = tokens.shape[1]

    values = tokens.astype(f32)
    normed = (values * lax.rsqrt(jnp.mean(values * values, axis=-1, keepdims=True) + EPS)).astype(bf)
    named = routes[:, :, None] == jnp.arange(count, dtype=jnp.int32)[None, None, :]
    weight = jnp.sum(jnp.where(named, route_weight[:, :, None], 0.0), axis=1)
    high = lax.reduce_precision(weight, 8, 7)
    extra = -(-2 * count // 128) * 128
    tail = jnp.concatenate(
        [high.astype(bf), (weight - high).astype(bf), jnp.zeros((tok_count, extra - 2 * count), bf)],
        axis=1,
    )
    rows_all = lax.all_gather(jnp.concatenate([normed, tail], axis=1), "fs", axis=0, tiled=True)

    gain_shared = lax.dynamic_slice_in_dim(
        norm_gain, fs_index * gate_shared.shape[0], gate_shared.shape[0], 0
    )
    gate_sw = lax.all_gather((gate_shared * gain_shared[:, None]).astype(bf), "fs", axis=0, tiled=True)
    up_sw = lax.all_gather((up_shared * gain_shared[:, None]).astype(bf), "fs", axis=0, tiled=True)
    down_sw = lax.all_gather(down_shared.astype(bf), "fs", axis=0, tiled=True)

    gain_cols = lax.dynamic_slice_in_dim(norm_gain, tp_index * cols, cols, 0)
    gate_w, up_w, down_w = exchange(
        dims,
        (gate_experts[0] * gain_cols[None, None, :]).astype(bf),
        (up_experts[0] * gain_cols[None, None, :]).astype(bf),
        down_experts[0].astype(bf),
    )

    x = rows_all[:, :width]
    w_all = (
        rows_all[:, width:width + count].astype(f32)
        + rows_all[:, width + count:width + 2 * count].astype(f32)
    )
    units = gate_w.shape[2]
    parts = []
    for g in range(n_gr):
        w_here = lax.dynamic_slice_in_dim(w_all, g * per_group + fs_index * held, held, 1)
        for k in range(held):
            gate = lax.dot_general(x, gate_w[g, k], (((1,), (1,)), ((), ())), preferred_element_type=f32)
            upper = lax.dot_general(x, up_w[g, k], (((1,), (1,)), ((), ())), preferred_element_type=f32)
            parts.append((jax.nn.silu(gate) * upper * w_here[:, k:k + 1]).astype(bf))
    hidden = jnp.stack(parts)
    hidden = lax.all_gather(hidden, "tp", axis=0, tiled=False)
    partial = jnp.zeros((), f32)
    down_flat = down_w.reshape(n_gr * held, n_tp, units, cols)
    for i in range(n_gr * held):
        for t in range(n_tp):
            partial = partial + jnp.dot(hidden[t, i], down_flat[i, t], preferred_element_type=f32)
    routed = lax.psum_scatter(partial.astype(bf), "fs", scatter_dimension=0, tiled=True)

    shared_hidden = (
        jax.nn.silu(jnp.dot(normed, gate_sw, preferred_element_type=f32))
        * jnp.dot(normed, up_sw, preferred_element_type=f32)
    ).astype(bf)
    shared_full = lax.all_gather(shared_hidden, "tp", axis=1, tiled=True)
    shared = jnp.dot(shared_full, down_sw, preferred_element_type=f32)
    mixed = (routed.astype(f32) + shared).astype(bf)
    return (mixed, gate_w, up_w, down_w, gate_sw, up_sw, down_sw)


def solution(mesh):
    return jax.shard_map(
        on_device,
        mesh=mesh,
        in_specs=(
            P(("gr", "fs"), None),
            P(("gr", "fs"), None),
            P(("gr", "fs"), None),
            P(),
            P("gr", None, "fs", "tp"),
            P("gr", None, "fs", "tp"),
            P("gr", None, "fs", "tp"),
            P("fs", "tp"),
            P("fs", "tp"),
            P("fs", "tp"),
        ),
        out_specs=(
            P(("gr", "fs"), "tp"),
            P(None, "fs", "tp", None),
            P(None, "fs", "tp", None),
            P(None, "fs", None, "tp"),
            P(None, "tp"),
            P(None, "tp"),
            P(None, "tp"),
        ),
        check_vma=False,
    )
```

time: 660 us -> 455 us (0.69); the launches traced: 651 us -> 454 us
  waiting for transfers between devices: 457 us -> 269 us
  Pallas kernels: 0 us -> 115 us
  local copies, waits for them, and re-layouts: 101 us -> 13.3 us
  starting transfers between devices: 36.5 us -> 0.42 us
    all_to_all x7 -> x0, waiting for transfers between devices: 242 us -> none  [the longest x1 85.7 us: on_device(): lax.all_to_all(send, 'fs', split_axis=0, concat_axis=0, tiled=True)]
    pallas_call x0 -> x1, Pallas kernels: none -> 115 us  [exchange(): pl.pallas_call(body, out_shape=(wide, wide, tall), in_specs=[pl.BlockSpec...]
    reduce_scatter x0 -> x1, waiting for transfers between devices: none -> 68.1 us  [on_device(): lax.psum_scatter(partial.astype(bf), 'fs', scatter_dimension=0, tiled=True)]
    all_to_all x7 -> x0, starting transfers between devices: 35.8 us -> none  [the longest x1 7.44 us: on_device(): lax.all_to_all(send, 'fs', split_axis=0, concat_axis=0, tiled=True)]
    all_to_all x12 -> x0, local copies, waits for them, and re-layouts: 35.2 us -> none  [the longest x3 9.61 us: on_device(): lax.all_to_all(gate_cols, 'tp', split_axis=2, concat_axis=3, tiled=True)]
    scatter x1 -> x0, local copies, waits for them, and re-layouts: 14.7 us -> none  [on_device(): send = jnp.zeros((total_slots, width), bf).at[slot].set(repeated)]
    all_gather x8 -> x5, waiting for transfers between devices: 214 us -> 201 us  [the longest x1 41.6 us: on_device(): lax.all_gather((up_shared * gain_shared[:, None]).astype(bf), 'fs', axis=...]
    gather x1 -> x0, local copies, waits for them, and re-layouts: 10 us -> none  [on_device(): returned.reshape(total_slots, cols)[slot].reshape(tok_count, top, cols)]
  transfers between devices with their start and end apart: 15 -> 6, of which waited for: 11 -> 6; matrix products, arithmetic and copies ran while one was open for 12% -> 4% of each run, Pallas kernels for 0% -> 25%
where the time goes in v1:
time: 455 us; the launch traced here: 454 us
  waiting for transfers between devices  269 us (59%)
  Pallas kernels  115 us (25%)
  matrix products  23.6 us (5%)
  between operations  14.4 us (3%)
  local copies, waits for them, and re-layouts  13.3 us (3%)
  other arithmetic  12.8 us (3%)
  blocking collectives  5.29 us (1%)
    pallas_call x1, Pallas kernels, exchange(): pl.pallas_call(body, out_shape=(wide, wide, tall), in_specs=[pl.BlockSpec...  115 us
    reduce_scatter x1, waiting for transfers between devices, on_device(): lax.psum_scatter(partial.astype(bf), 'fs', scatter_dimension=0, tiled=True)  68.1 us
    all_gather x1, waiting for transfers between devices, on_device(): lax.all_gather((up_shared * gain_shared[:, None]).astype(bf), 'fs', axis=...  41.6 us
    all_gather x1, waiting for transfers between devices, on_device(): down_sw = lax.all_gather(down_shared.astype(bf), 'fs', axis=0, tiled=True)  41.6 us
    all_gather x1, waiting for transfers between devices, on_device(): lax.all_gather(jnp.concatenate([normed, tail], axis=1), 'fs', axis=0, til...  41.6 us
    all_gather x1, waiting for transfers between devices, on_device(): hidden = lax.all_gather(hidden, 'tp', axis=0, tiled=False)  40 us
    all_gather x1, waiting for transfers between devices, on_device(): lax.all_gather((gate_shared * gain_shared[:, None]).astype(bf), 'fs', axi...  36.1 us
    unnamed x40, local copies, waits for them, and re-layouts  11 us
  transfers between devices with their start and end apart: 6, of which 6 were waited for; matrix products, arithmetic and copies ran while one was open for 4% of the time, Pallas kernels for 25%

profile of v1, /device:TPU:0, one launch (start us, length us, event | category | flops | bytes accessed | tf_op | source)
XLA Modules:
  0.0 454.5 jit_solution(18316854848922227621)
XLA Ops:
  7.2 0.0 all-gather.7.cloned.1.call-start
  7.2 1.4 fusion.34
  8.6 1.5 fusion.35
  10.2 0.1 copy.23
  10.3 0.1 copy.24
  10.4 1.1 concatenate.3
  11.5 0.0 all-gather.15.cloned.1.call-start
  11.6 1.1 convert_bitcast_fusion.refs_2_
  12.7 0.8 copy-done.8
  13.6 3.5 fusion.32
  17.0 115.3 %shard_map.153 = (bf16[2,1,256,2048]{3,2,1,0:T(8,128)(2,1)}, bf16[2,1,256,2048]{3,2,1,0:T(8,128)(2,1)}, bf16[2,1,512,1024]{3,2,1,0:T(8,128)(2,1)}) custom-call(bf16[8,64,1024]{2,1,0:T(8,128)(2,1)} %get-tuple-element.18.refs_0_, bf16[8,64,1024]{2,1,0:T(8,128)(2,1)} %get-tuple-element.17.refs_1_, bf16[8,64,1024]{2,1,0:T(8,128)(2,1)} %convert_bitcast_fusion.refs_2_), custom_call_target="tpu_custom_call" | custom-call | bytes 314572800 | tf_op jit(solution)/shard_map/pallas_call | solution.py:173
  132.3 41.6 %all-gather.7.cloned.1.call-done = bf16[1536,2176]{1,0:T(8,128)(2,1)} async-done(((bf16[192,2176]{1,0:T(8,128)(2,1)}), bf16[1536,2176]{1,0:T(8,128)(2,1)}) %all-gather.7.cloned.1.call-update) | async-done | bytes 6684688 | tf_op jit(solution)/shard_map/all_gather | solution.py:213
  173.9 1.4 convert_add_fusion
  175.3 0.9 dynamic-slice_reduce_fusion.1
  176.3 5.0 %fusion.6 = f32[1536,256]{1,0:T(8,128)S(1)} fusion(bf16[1536,2176]{1,0:T(8,128)(2,1)} %all-gather.7.cloned.1.call-done, bf16[2,1,256,2048]{3,2,1,0:T(8,128)(2,1)S(1)} %copy-done.7), kind=kOutput, calls=%fused_computation.7 | convolution fusion | flops 1610612736 | bytes 8912896 | tf_op jit(solution)/shard_map/dot_general | solution.py:240
  181.3 1.9 fusion.2
  183.2 2.1 fusion.26
  185.3 2.1 fusion.29
  187.4 1.3 pad_maximum_fusion
  188.7 0.0 all-gather.9.cloned.1.call-start
  188.8 0.1 dynamic_slice.15
  188.9 1.9 multiply_convert_fusion.1
  190.8 0.0 all-gather.11.cloned.1.call-start
  190.8 0.5 all-gather.11.cloned.1.call-update
  191.4 0.0 all-gather.13.cloned.1.call-start
  191.4 0.7 convert_element_type.73
  192.1 0.2 reduce-scatter.2.cloned.1.call-start
  192.3 40.0 %all-gather.15.cloned.1.call-done = bf16[4,1536,256]{2,1,0:T(8,128)(2,1)} async-done(((bf16[2,1536,256]{2,1,0:T(8,128)(2,1)}), bf16[4,1536,256]{2,1,0:T(8,128)(2,1)}) %all-gather.15.cloned.1.call-update) | async-done | bytes 3145744 | tf_op jit(solution)/shard_map/all_gather | solution.py:244
  232.3 2.3 fusion.47
  234.6 1.0 fusion.48
  235.6 1.0 fusion.46
  236.6 2.7 add_convert_fusion
  239.3 36.1 %all-gather.9.cloned.1.call-done = bf16[2048,256]{1,0:T(8,128)(2,1)} async-done(((bf16[256,256]{1,0:T(8,128)(2,1)}), bf16[2048,256]{1,0:T(8,128)(2,1)}) %all-gather.9.cloned.1.call-update) | async-done | bytes 1048592 | tf_op jit(solution)/shard_map/all_gather | solution.py:218
  275.3 41.6 %all-gather.11.cloned.1.call-done = bf16[2048,256]{1,0:T(8,128)(2,1)} async-done(((bf16[256,256]{1,0:T(8,128)(2,1)}), bf16[2048,256]{1,0:T(8,128)(2,1)}) %all-gather.11.cloned.1.call-update) | async-done | bytes 1048592 | tf_op jit(solution)/shard_map/all_gather | solution.py:219
  316.9 41.6 %all-gather.13.cloned.1.call-done = bf16[512,1024]{1,0:T(8,128)(2,1)} async-done(((bf16[64,1024]{1,0:T(8,128)(2,1)}), bf16[512,1024]{1,0:T(8,128)(2,1)}) %all-gather.13.cloned.1.call-update) | async-done | bytes 1048592 | tf_op jit(solution)/shard_map/all_gather | solution.py:220
  358.5 1.6 fusion.50
  360.1 1.6 fusion.37
  361.7 5.3 %all_gather.26 = bf16[192,512]{1,0:T(8,128)(2,1)S(1)} all-gather(bf16[192,256]{1,0:T(8,128)(2,1)S(1)} %fusion.37), channel_id=1, replica_groups=mesh['gr'=2,'fs'=8,'tp'=2] {'tp'}, dimensions={1}, use_global_device_ids=true | all-gather | bytes 294912 | tf_op jit(solution)/shard_map/all_gather | solution.py:256
  367.0 68.1 %reduce-scatter.2.cloned.1.call-done = bf16[192,1024]{1,0:T(8,128)(2,1)} async-done(((bf16[1536,1024]{1,0:T(8,128)(2,1)}), bf16[192,1024]{1,0:T(8,128)(2,1)}) %reduce-scatter.2.cloned.1.call-update) | async-done | bytes 393232 | tf_op jit(solution)/shard_map/reduce_scatter | solution.py:250
  435.1 2.4 fusion.36
  437.5 3.3 copy.31
  440.8 1.3 copy.32
  442.1 1.3 copy.33
  443.5 0.6 copy-done.2
  444.1 1.0 copy.34
  445.1 0.6 copy-done.9
  445.7 1.0 copy.35
  446.7 1.0 copy.36
  (43 shorter events, 0.2 us)
Async XLA Ops:
  7.2 2.9 copy-start.14
  7.2 2.9 copy-start.13
  7.2 166.7 %all-gather.7.cloned.1.call-start = ((), (), s32[]{:S(2)}) async-start(), calls=%async_computation.1 | async-start | bytes 7520256 | tf_op jit(solution)/shard_map/all_gather | solution.py:213
  8.6 3.0 copy-start.4
  11.5 220.8 %all-gather.15.cloned.1.call-start = ((), (), s32[]{:S(2)}) async-start(), calls=%async_computation.6 | async-start | bytes 4718592 | tf_op jit(solution)/shard_map/all_gather | solution.py:244
  11.6 2.0 copy-start.8
  11.6 2.0 dynamic-slice-start
  132.3 43.9 %copy-start.7 = (bf16[2,1,256,2048]{3,2,1,0:T(8,128)(2,1)S(1)}, bf16[2,1,256,2048]{3,2,1,0:T(8,128)(2,1)}, u32[]{:S(2)}) copy-start(bf16[2,1,256,2048]{3,2,1,0:T(8,128)(2,1)} %get-tuple-element.29) | copy-start | bytes 6291460
  175.3 6.0 %slice-start = ((s8[6684672]{0:T(1024)(128)(4,1)}), s8[4194304]{0:T(1024)(128)(4,1)S(1)}, s32[]{:S(2)}) async-start(s8[6684672]{0:T(1024)(128)(4,1)} %bitcast.66), calls=%async_computation.7 | async-start | bytes 8388608
  176.2 5.0 %slice-start.1 = ((s8[6684672]{0:T(1024)(128)(4,1)}), s8[2490368]{0:T(1024)(128)(4,1)S(1)}, s32[]{:S(2)}) async-start(s8[6684672]{0:T(1024)(128)(4,1)} %bitcast.66), calls=%async_computation.8 | async-start | bytes 4980736
  181.3 1.9 copy-start.5
  187.4 1.4 copy-start.12
  187.4 1.5 copy-start.11
  188.7 2.7 copy-start.10
  188.7 43.6 %copy-start = (bf16[2,1,512,1024]{3,2,1,0:T(8,128)(2,1)S(1)}, bf16[2,1,512,1024]{3,2,1,0:T(8,128)(2,1)}, u32[]{:S(2)}) copy-start(bf16[2,1,512,1024]{3,2,1,0:T(8,128)(2,1)} %get-tuple-element.31) | copy-start | bytes 6291460
  188.7 86.6 %all-gather.9.cloned.1.call-start = ((), (), s32[]{:S(2)}) async-start(), calls=%async_computation.3 | async-start | bytes 1179648 | tf_op jit(solution)/shard_map/all_gather | solution.py:218
  190.8 126.1 %all-gather.11.cloned.1.call-start = ((), (), s32[]{:S(2)}) async-start(), calls=%async_computation.4 | async-start | bytes 1179648 | tf_op jit(solution)/shard_map/all_gather | solution.py:219
  191.4 167.1 %all-gather.13.cloned.1.call-start = ((), (), s32[]{:S(2)}) async-start(), calls=%async_computation.5 | async-start | bytes 1179648 | tf_op jit(solution)/shard_map/all_gather | solution.py:220
  192.1 242.9 %reduce-scatter.2.cloned.1.call-start = ((), (), s32[]{:S(2)}) async-start(), calls=%async_computation.2 | async-start | bytes 3538944 | tf_op jit(solution)/shard_map/reduce_scatter | solution.py:250
  232.3 2.3 copy-start.1
  437.5 3.3 copy-start.6
  442.1 2.0 copy-start.2
  444.1 1.6 copy-start.9
  444.1 2.6 copy-start.3
Sparse Core Ops, SparseCore 0:
  11.6 162.1 all-gather.6
  188.9 43.4 all-gather.14
  235.0 40.2 all-gather.8
  277.9 38.9 all-gather.10
  319.5 38.9 all-gather.12
  361.9 73.0 reduce-scatter.1

commit v2 on v1

v2 whole, which is shorter than its diff:
```python
import functools

import jax
import jax.numpy as jnp
from jax import lax
from jax.experimental import pallas as pl
from jax.experimental.pallas import tpu as pltpu
from jax.sharding import PartitionSpec as P

EPS = 1e-06
MESH = pl.DeviceIdType.MESH


def greet_group(dims, gr, fs, tp, barrier):
    n_gr, n_fs, n_tp = dims

    def greet(i, carry):
        f, t = i // n_tp, i % n_tp

        @pl.when((f != fs) | (t != tp))
        def _():
            pl.semaphore_signal(barrier, inc=1, device_id=(gr, f, t), device_id_type=MESH)
        return carry

    lax.fori_loop(0, n_fs * n_tp, greet, 0)
    for p in range(1, n_gr):
        pl.semaphore_signal(
            barrier, inc=1, device_id=((gr + p) % n_gr, fs, tp), device_id_type=MESH
        )
    pl.semaphore_wait(barrier, n_fs * n_tp - 1 + n_gr - 1)


def forward(n_gr, block, s_sem, r_sem, p):
    gr, fs, tp = lax.axis_index("gr"), lax.axis_index("fs"), lax.axis_index("tp")
    return pltpu.make_async_remote_copy(
        src_ref=block, dst_ref=block, send_sem=s_sem, recv_sem=r_sem,
        device_id=((gr + p) % n_gr, fs, tp), device_id_type=MESH,
    )


def wide_kernel(dims, g_loc, u_loc, g_out, u_out, send, recv, own, f_send, f_recv):
    n_gr, n_fs, n_tp = dims
    gr, fs, tp = lax.axis_index("gr"), lax.axis_index("fs"), lax.axis_index("tp")
    held = g_loc.shape[0] // n_fs
    rows, cols = g_loc.shape[1], g_loc.shape[2]
    per = g_out.shape[2] // rows
    greet_group(dims, gr, fs, tp, pltpu.get_barrier_semaphore())
    to_tp = fs // per

    def place(out):
        return out.at[gr, :, pl.ds(pl.multiple_of((fs % per) * rows, rows), rows),
                      pl.ds(pl.multiple_of(tp * cols, cols), cols)]

    def wide(loc, out, m, d):
        k = (fs + d) % n_fs
        return pltpu.make_async_remote_copy(
            src_ref=loc.at[pl.ds(k * held, held)], dst_ref=place(out),
            send_sem=send.at[m, d], recv_sem=recv.at[m, fs % per, tp],
            device_id=(gr, k, to_tp), device_id_type=MESH,
        )

    def wide_own(loc, out, m):
        return pltpu.make_async_copy(loc.at[pl.ds(fs * held, held)], place(out), own.at[m])

    def block(out, g, j, t):
        return out.at[g, :, pl.ds(j * rows, rows), pl.ds(t * cols, cols)]

    pairs = ((g_loc, g_out, 0), (u_loc, u_out, 1))
    for loc, out, m in pairs:
        for d in range(1, n_fs):
            wide(loc, out, m, d).start()

        @pl.when(to_tp == tp)
        def _():
            wide_own(loc, out, m).start()

        @pl.when(to_tp != tp)
        def _():
            wide(loc, out, m, 0).start()
    for loc, out, m in pairs:
        for j in range(per):
            for t in range(n_tp):
                here = (tp * per + j == fs) & (tp == t)
                part = block(out, gr, j, t)

                @pl.when(here)
                def _():
                    wide_own(loc, out, m).wait()

                @pl.when(jnp.logical_not(here))
                def _():
                    forward(n_gr, part, recv.at[m, j, t], recv.at[m, j, t], 1).wait_recv()
                for p in range(1, n_gr):
                    forward(n_gr, part, f_send.at[m, j, t, p - 1], f_recv.at[m, j, t, p - 1], p).start()
    for loc, out, m in pairs:
        for d in range(1, n_fs):
            wide(loc, out, m, d).wait_send()

        @pl.when(to_tp != tp)
        def _():
            wide(loc, out, m, 0).wait_send()
        for j in range(per):
            for t in range(n_tp):
                for p in range(1, n_gr):
                    sems = f_send.at[m, j, t, p - 1], f_recv.at[m, j, t, p - 1]
                    forward(n_gr, block(out, gr, j, t), *sems, p).wait_send()
                    forward(n_gr, block(out, (gr + n_gr - p) % n_gr, j, t), *sems, p).wait_recv()


def tall_kernel(dims, d_loc, d_out, send, recv, own, f_send, f_recv):
    n_gr, n_fs, n_tp = dims
    gr, fs, tp = lax.axis_index("gr"), lax.axis_index("fs"), lax.axis_index("tp")
    held = d_loc.shape[0] // n_fs
    rows = d_loc.shape[1]
    greet_group(dims, gr, fs, tp, pltpu.get_barrier_semaphore())

    def block(g, s):
        start = s * rows if isinstance(s, int) else pl.multiple_of(s * rows, rows)
        return d_out.at[g, :, pl.ds(start, rows), :]

    def tall(d):
        k = (fs + d) % n_fs
        return pltpu.make_async_remote_copy(
            src_ref=d_loc.at[pl.ds(k * held, held)], dst_ref=block(gr, fs),
            send_sem=send.at[d], recv_sem=recv.at[fs],
            device_id=(gr, k, tp), device_id_type=MESH,
        )

    mine = pltpu.make_async_copy(d_loc.at[pl.ds(fs * held, held)], block(gr, fs), own)
    for d in range(1, n_fs):
        tall(d).start()
    mine.start()
    for s in range(n_fs):
        @pl.when(s == fs)
        def _():
            mine.wait()

        @pl.when(s != fs)
        def _():
            forward(n_gr, block(gr, s), recv.at[s], recv.at[s], 1).wait_recv()
        for p in range(1, n_gr):
            forward(n_gr, block(gr, s), f_send.at[s, p - 1], f_recv.at[s, p - 1], p).start()
    for d in range(1, n_fs):
        tall(d).wait_send()
    for s in range(n_fs):
        for p in range(1, n_gr):
            sems = f_send.at[s, p - 1], f_recv.at[s, p - 1]
            forward(n_gr, block(gr, s), *sems, p).wait_send()
            forward(n_gr, block((gr + n_gr - p) % n_gr, s), *sems, p).wait_recv()


def gather_kernel(dims, inner, number, *refs):
    n_gr, n_fs, n_tp = dims
    gr, fs, tp = lax.axis_index("gr"), lax.axis_index("fs"), lax.axis_index("tp")
    ins, outs = refs[:number], refs[number:2 * number]
    z_send, z_recv, y_send, y_recv, own = refs[2 * number:]
    nz = n_fs // inner
    z, y = fs // inner, fs % inner
    barrier = pltpu.get_barrier_semaphore()

    def when_next(way, act):
        pl.when(z < nz - 1 if way == 0 else z > 0)(act)

    def beside(way):
        return (gr, (z + 1 if way == 0 else z - 1) * inner + y, tp)

    for q in range(1, inner):
        pl.semaphore_signal(barrier, inc=1, device_id=(gr, z * inner + (y + q) % inner, tp), device_id_type=MESH)
    for way in (0, 1):
        when_next(way, lambda way=way: pl.semaphore_signal(
            barrier, inc=1, device_id=beside(way), device_id_type=MESH))
    peers = inner - 1 + (z > 0).astype(jnp.int32) + (z < nz - 1).astype(jnp.int32)
    pl.semaphore_wait(barrier, peers)

    def block(m, zz, yy):
        rows = ins[m].shape[0]
        return outs[m].at[pl.ds(pl.multiple_of((zz * inner + yy) * rows, rows), rows), :]

    def at(way, d):
        return z - d if way == 0 else z + d

    def z_copy(m, way, d):
        return pltpu.make_async_remote_copy(
            src_ref=ins[m] if d == 0 else block(m, at(way, d), y), dst_ref=block(m, at(way, d), y),
            send_sem=z_send.at[m, way, d], recv_sem=z_recv.at[m, way, d],
            device_id=beside(way), device_id_type=MESH,
        )

    def z_landed(m, way, d):
        part = block(m, at(way, d), y)
        pltpu.make_async_remote_copy(
            src_ref=part, dst_ref=part, send_sem=z_send.at[m, way, d - 1],
            recv_sem=z_recv.at[m, way, d - 1], device_id=beside(way), device_id_type=MESH,
        ).wait_recv()

    def y_copy(m, q, way, d, source):
        part = block(m, at(way, d), source)
        i = d + way * (nz - 1) if d else 0
        return pltpu.make_async_remote_copy(
            src_ref=ins[m] if d == 0 else part, dst_ref=part,
            send_sem=y_send.at[m, q - 1, i], recv_sem=y_recv.at[m, q - 1, i],
            device_id=(gr, z * inner + (y + q) % inner, tp), device_id_type=MESH,
        )

    def own_copy(m):
        return pltpu.make_async_copy(ins[m], block(m, z, y), own.at[m])

    def steps(d, way, act):
        if d == 0:
            act()
        else:
            pl.when(z - d >= 0 if way == 0 else z + d < nz)(act)

    places = [(0, 0)] + [(d, way) for d in range(1, nz) for way in (0, 1)]
    for m in range(number):
        for way in (0, 1):
            when_next(way, lambda m=m, way=way: z_copy(m, way, 0).start())
        for q in range(1, inner):
            y_copy(m, q, 0, 0, y).start()
    for m in range(number):
        own_copy(m).start()
    for d, way in places[1:]:
        def pass_on(d=d, way=way):
            for m in range(number):
                z_landed(m, way, d)
                if d < nz - 1:
                    when_next(way, lambda: z_copy(m, way, d).start())
                for q in range(1, inner):
                    y_copy(m, q, way, d, y).start()
        steps(d, way, pass_on)
    for m in range(number):
        for way in (0, 1):
            when_next(way, lambda m=m, way=way: z_copy(m, way, 0).wait_send())
    for d, way in places:
        def finish(d=d, way=way):
            for m in range(number):
                if 0 < d < nz - 1:
                    when_next(way, lambda: z_copy(m, way, d).wait_send())
                for q in range(1, inner):
                    y_copy(m, q, way, d, y).wait_send()
                    y_copy(m, q, way, d, (y + inner - q) % inner).wait_recv()
        steps(d, way, finish)
    for m in range(number):
        own_copy(m).wait()


def call(body, outs, sems, ident, work, *args):
    return pl.pallas_call(
        body,
        out_shape=outs,
        in_specs=[pl.BlockSpec(memory_space=pl.ANY)] * len(args),
        out_specs=tuple(pl.BlockSpec(memory_space=pl.ANY) for _ in outs),
        scratch_shapes=[pltpu.SemaphoreType.DMA(shape) for shape in sems],
        compiler_params=pltpu.CompilerParams(collective_id=ident, has_side_effects=True),
        cost_estimate=pl.CostEstimate(flops=0, bytes_accessed=work, transcendentals=0),
    )(*args)


def exchange_wide(dims, g_loc, u_loc):
    n_gr, n_fs, n_tp = dims
    count, rows, cols = g_loc.shape
    per = n_fs // n_tp
    out = jax.ShapeDtypeStruct((n_gr, count // n_fs, per * rows, n_tp * cols), g_loc.dtype)
    halves = (2, per, n_tp, n_gr - 1)
    return call(
        functools.partial(wide_kernel, dims), (out, out),
        [(2, n_fs), (2, per, n_tp), (2,), halves, halves], 1, 200 << 20, g_loc, u_loc,
    )


def exchange_tall(dims, d_loc):
    n_gr, n_fs, n_tp = dims
    count, rows, cols = d_loc.shape
    out = jax.ShapeDtypeStruct((n_gr, count // n_fs, n_fs * rows, cols), d_loc.dtype)
    return call(
        functools.partial(tall_kernel, dims), (out,),
        [(n_fs,), (n_fs,), (), (n_fs, n_gr - 1), (n_fs, n_gr - 1)], 2, 100 << 20, d_loc,
    )[0]


def gather_fs(dims, ident, work, *arrays):
    n_fs = dims[1]
    inner = 2 if n_fs % 2 == 0 else 1
    nz = n_fs // inner
    number = len(arrays)
    outs = tuple(jax.ShapeDtypeStruct((n_fs * a.shape[0], a.shape[1]), a.dtype) for a in arrays)
    chain = (number, 2, max(1, nz - 1))
    across = (number, max(1, inner - 1), 2 * nz - 1)
    return call(
        functools.partial(gather_kernel, dims, inner, number), outs,
        [chain, chain, across, across, (number,)], ident, work, *arrays,
    )


def on_device(tokens, routes, route_weight, norm_gain, gate_experts, up_experts, down_experts,
              gate_shared, up_shared, down_shared):
    bf = jnp.bfloat16
    f32 = jnp.float32
    dims = (lax.axis_size("gr"), lax.axis_size("fs"), lax.axis_size("tp"))
    n_gr, n_fs, n_tp = dims
    fs_index = lax.axis_index("fs")
    tp_index = lax.axis_index("tp")
    cols = gate_experts.shape[3]
    per_group = gate_experts.shape[1]
    count = per_group * n_gr
    held = per_group // n_fs
    tok_count, top = routes.shape
    width = tokens.shape[1]

    values = tokens.astype(f32)
    normed = (values * lax.rsqrt(jnp.mean(values * values, axis=-1, keepdims=True) + EPS)).astype(bf)
    named = routes[:, :, None] == jnp.arange(count, dtype=jnp.int32)[None, None, :]
    weight = jnp.sum(jnp.where(named, route_weight[:, :, None], 0.0), axis=1)
    high = lax.reduce_precision(weight, 8, 7)
    extra = -(-2 * count // 128) * 128
    tail = jnp.concatenate(
        [high.astype(bf), (weight - high).astype(bf), jnp.zeros((tok_count, extra - 2 * count), bf)],
        axis=1,
    )
    rows_all = lax.all_gather(jnp.concatenate([normed, tail], axis=1), "fs", axis=0, tiled=True)

    gain_shared = lax.dynamic_slice_in_dim(
        norm_gain, fs_index * gate_shared.shape[0], gate_shared.shape[0], 0
    )
    shared_here = (
        (gate_shared * gain_shared[:, None]).astype(bf),
        (up_shared * gain_shared[:, None]).astype(bf),
        down_shared.astype(bf),
    )

    gain_cols = lax.dynamic_slice_in_dim(norm_gain, tp_index * cols, cols, 0)
    gate_w, up_w = exchange_wide(
        dims,
        (gate_experts[0] * gain_cols[None, None, :]).astype(bf),
        (up_experts[0] * gain_cols[None, None, :]).astype(bf),
    )

    x = rows_all[:, :width]
    w_all = (
        rows_all[:, width:width + count].astype(f32)
        + rows_all[:, width + count:width + 2 * count].astype(f32)
    )
    units = gate_w.shape[2]
    parts = []
    for g in range(n_gr):
        w_here = lax.dynamic_slice_in_dim(w_all, g * per_group + fs_index * held, held, 1)
        for k in range(held):
            gate = lax.dot_general(x, gate_w[g, k], (((1,), (1,)), ((), ())), preferred_element_type=f32)
            upper = lax.dot_general(x, up_w[g, k], (((1,), (1,)), ((), ())), preferred_element_type=f32)
            parts.append((jax.nn.silu(gate) * upper * w_here[:, k:k + 1]).astype(bf))
    hidden = jnp.stack(parts)
    hidden, down_local = lax.optimization_barrier((hidden, down_experts[0].astype(bf)))
    down_w = exchange_tall(dims, down_local)
    hidden = lax.all_gather(hidden, "tp", axis=0, tiled=False)
    partial = jnp.zeros((), f32)
    down_flat = down_w.reshape(n_gr * held, n_tp, units, cols)
    for i in range(n_gr * held):
        for t in range(n_tp):
            partial = partial + jnp.dot(hidden[t, i], down_flat[i, t], preferred_element_type=f32)
    partial, shared_here = lax.optimization_barrier((partial.astype(bf), shared_here))
    gate_sw, up_sw, down_sw = gather_fs(dims, 3, 60 << 20, *shared_here)
    routed = lax.psum_scatter(partial, "fs", scatter_dimension=0, tiled=True)

    shared_hidden = (
        jax.nn.silu(jnp.dot(normed, gate_sw, preferred_element_type=f32))
        * jnp.dot(normed, up_sw, preferred_element_type=f32)
    ).astype(bf)
    shared_full = lax.all_gather(shared_hidden, "tp", axis=1, tiled=True)
    shared = jnp.dot(shared_full, down_sw, preferred_element_type=f32)
    mixed = (routed.astype(f32) + shared).astype(bf)
    return (mixed, gate_w, up_w, down_w, gate_sw, up_sw, down_sw)


def solution(mesh):
    return jax.shard_map(
        on_device,
        mesh=mesh,
        in_specs=(
            P(("gr", "fs"), None),
            P(("gr", "fs"), None),
            P(("gr", "fs"), None),
            P(),
            P("gr", None, "fs", "tp"),
            P("gr", None, "fs", "tp"),
            P("gr", None, "fs", "tp"),
            P("fs", "tp"),
            P("fs", "tp"),
            P("fs", "tp"),
        ),
        out_specs=(
            P(("gr", "fs"), "tp"),
            P(None, "fs", "tp", None),
            P(None, "fs", "tp", None),
            P(None, "fs", None, "tp"),
            P(None, "tp"),
            P(None, "tp"),
            P(None, "tp"),
        ),
        check_vma=False,
    )
```

time: 455 us -> 331 us (0.73)
  waiting for transfers between devices: 269 us -> 107 us
  Pallas kernels: 115 us -> 156 us
    all_gather x3 -> x0, waiting for transfers between devices: 119 us -> none  [the longest x1 41.6 us: on_device(): lax.all_gather((up_shared * gain_shared[:, None]).astype(bf), 'fs', axis=...]
    reduce_scatter x1, waiting for transfers between devices: 68.1 us -> 17.6 us  [on_device(): routed = lax.psum_scatter(partial, 'fs', scatter_dimension=0, tiled=True)]
    pallas_call x1 -> x3, Pallas kernels: 115 us -> 156 us  [call(): pl.pallas_call(body, out_shape=outs, in_specs=[pl.BlockSpec(memory_space=...]
    all_gather x1, waiting for transfers between devices: 41.6 us -> 69.3 us  [on_device(): lax.all_gather(jnp.concatenate([normed, tail], axis=1), 'fs', axis=0, til...]
    all_gather x1, waiting for transfers between devices: 40 us -> 19.8 us  [on_device(): hidden = lax.all_gather(hidden, 'tp', axis=0, tiled=False)]
    unnamed x40 -> x42, local copies, waits for them, and re-layouts: 11 us -> 10.7 us
  transfers between devices with their start and end apart: 6 -> 3, of which waited for: 6 -> 3; matrix products, arithmetic and copies ran while one was open for 4% -> 3% of each run, Pallas kernels for 25% -> 47%
where the time goes in v2:
time: 331 us; the launch traced here: 330 us
  Pallas kernels  156 us (47%)
  waiting for transfers between devices  107 us (32%)
  matrix products  23.8 us (7%)
  between operations  14.1 us (4%)
  local copies, waits for them, and re-layouts  13 us (4%)
  other arithmetic  11.6 us (4%)
  blocking collectives  5.29 us (2%)
    pallas_call x3, Pallas kernels, call(): pl.pallas_call(body, out_shape=outs, in_specs=[pl.BlockSpec(memory_space=...  156 us
    all_gather x1, waiting for transfers between devices, on_device(): lax.all_gather(jnp.concatenate([normed, tail], axis=1), 'fs', axis=0, til...  69.3 us
    all_gather x1, waiting for transfers between devices, on_device(): hidden = lax.all_gather(hidden, 'tp', axis=0, tiled=False)  19.8 us
    reduce_scatter x1, waiting for transfers between devices, on_device(): routed = lax.psum_scatter(partial, 'fs', scatter_dimension=0, tiled=True)  17.6 us
    unnamed x42, local copies, waits for them, and re-layouts  10.7 us
    dot_general x4, matrix products, on_device(): jnp.dot(hidden[t, i], down_flat[i, t], preferred_element_type=f32)  7.07 us
    dot_general x2, matrix products, on_device(): lax.dot_general(x, gate_w[g, k], (((1,), (1,)), ((), ())), preferred_elem...  6.91 us
  transfers between devices with their start and end apart: 3, of which 3 were waited for; matrix products, arithmetic and copies ran while one was open for 3% of the time, Pallas kernels for 47%

profile of v2, /device:TPU:0, one launch (start us, length us, event | category | flops | bytes accessed | tf_op | source)
XLA Modules:
  0.0 330.3 jit_solution(7086527797900964982)
XLA Ops:
  7.2 0.0 all-gather.4.cloned.1.call-start
  7.2 1.4 fusion.34
  8.6 0.0 copy-start.8
  8.6 1.5 fusion.35
  10.2 0.1 copy.23
  10.3 0.1 copy.24
  10.4 1.1 concatenate.3
  11.5 0.0 all-gather.4.cloned.1.call-update
  11.5 0.0 all-gather.6.cloned.1.call-start
  11.6 3.5 %fusion.32 = (bf16[8,64,1024]{2,1,0:T(8,128)(2,1)}, bf16[8,64,1024]{2,1,0:T(8,128)(2,1)}) fusion(f32[1,8,64,1024]{3,2,1,0:T(8,128)S(1)} %copy-done.8, f32[1024]{0:T(1024)S(1)} %dynamic_slice.12, f32[1,8,64,1024]{3,2,1,0:T(8,128)} %param.14), kind=kLoop, calls=%fused_computation.18 | loop fusion | flops 2097152 | bytes 6295552 | tf_op jit(solution)/shard_map/convert_element_type | solution.py:335
  15.1 68.4 %shard_map.153 = (bf16[2,1,256,2048]{3,2,1,0:T(8,128)(2,1)}, bf16[2,1,256,2048]{3,2,1,0:T(8,128)(2,1)}) custom-call(bf16[8,64,1024]{2,1,0:T(8,128)(2,1)} %get-tuple-element.34.g_loc, bf16[8,64,1024]{2,1,0:T(8,128)(2,1)} %get-tuple-element.33.u_loc), custom_call_target="tpu_custom_call" | custom-call | bytes 209715200 | tf_op jit(solution)/shard_map/pallas_call | solution.py:248
  83.5 1.1 convert_bitcast_fusion.d_loc
  84.7 69.3 %all-gather.4.cloned.1.call-done = bf16[1536,2176]{1,0:T(8,128)(2,1)} async-done(((bf16[192,2176]{1,0:T(8,128)(2,1)}), bf16[1536,2176]{1,0:T(8,128)(2,1)}) %all-gather.4.cloned.1.call-update) | async-done | bytes 6684688 | tf_op jit(solution)/shard_map/all_gather | solution.py:320
  153.9 1.3 convert_add_fusion
  155.3 0.9 dynamic-slice_reduce_fusion.1
  156.2 5.0 %fusion.6 = f32[1536,256]{1,0:T(8,128)S(1)} fusion(bf16[1536,2176]{1,0:T(8,128)(2,1)} %all-gather.4.cloned.1.call-done, bf16[2,1,256,2048]{3,2,1,0:T(8,128)(2,1)S(1)} %copy-done.7), kind=kOutput, calls=%fused_computation.7 | convolution fusion | flops 1610612736 | bytes 8912896 | tf_op jit(solution)/shard_map/dot_general | solution.py:348
  161.2 1.9 fusion.2
  163.2 2.1 fusion.26
  165.3 2.1 fusion.29
  167.4 0.0 copy-start.11
  167.4 1.3 pad_maximum_fusion
  168.7 0.0 all-gather.6.cloned.1.call-update
  168.7 0.2 reduce-scatter.2.cloned.1.call-start
  168.9 0.1 dynamic_slice.15
  169.0 0.7 convert_element_type.72.refs_2_
  169.7 0.8 multiply_convert_fusion
  170.5 21.6 %shard_map.154 = bf16[2,1,512,1024]{3,2,1,0:T(8,128)(2,1)} custom-call(bf16[8,64,1024]{2,1,0:T(8,128)(2,1)} %convert_bitcast_fusion.d_loc), custom_call_target="tpu_custom_call" | custom-call | bytes 104857600 | tf_op jit(solution)/shard_map/pallas_call | solution.py:248
  192.1 19.8 %all-gather.6.cloned.1.call-done = bf16[4,1536,256]{2,1,0:T(8,128)(2,1)} async-done(((bf16[2,1536,256]{2,1,0:T(8,128)(2,1)}), bf16[4,1536,256]{2,1,0:T(8,128)(2,1)}) %all-gather.6.cloned.1.call-update) | async-done | bytes 3145744 | tf_op jit(solution)/shard_map/all_gather | solution.py:354
  211.9 2.4 fusion.47
  214.3 0.5 copy-done.1
  214.8 1.0 fusion.48
  215.8 1.0 fusion.46
  216.8 2.7 add_convert_fusion
  219.5 0.0 reduce-scatter.2.cloned.1.call-update
  219.5 65.5 %shard_map.155 = (bf16[2048,256]{1,0:T(8,128)(2,1)}, bf16[2048,256]{1,0:T(8,128)(2,1)}, bf16[512,1024]{1,0:T(8,128)(2,1)}) custom-call(bf16[256,256]{1,0:T(8,128)(2,1)} %get-tuple-element.23.refs_0_, bf16[256,256]{1,0:T(8,128)(2,1)} %get-tuple-element.24.refs_1_, bf16[64,1024]{1,0:T(8,128)(2,1)} %convert_element_type.72.refs_2_), custom_call_target="tpu_custom_call" | custom-call | bytes 62914560 | tf_op jit(solution)/shard_map/pallas_call | solution.py:248
  285.1 1.6 fusion.50
  286.7 1.6 fusion.37
  288.3 5.3 %all_gather.15 = bf16[192,512]{1,0:T(8,128)(2,1)S(1)} all-gather(bf16[192,256]{1,0:T(8,128)(2,1)S(1)} %fusion.37), channel_id=1, replica_groups=mesh['gr'=2,'fs'=8,'tp'=2] {'tp'}, dimensions={1}, use_global_device_ids=true | all-gather | bytes 294912 | tf_op jit(solution)/shard_map/all_gather | solution.py:368
  293.6 17.6 %reduce-scatter.2.cloned.1.call-done = bf16[192,1024]{1,0:T(8,128)(2,1)} async-done(((bf16[1536,1024]{1,0:T(8,128)(2,1)}), bf16[192,1024]{1,0:T(8,128)(2,1)}) %reduce-scatter.2.cloned.1.call-update) | async-done | bytes 393232 | tf_op jit(solution)/shard_map/reduce_scatter | solution.py:362
  311.2 2.4 fusion.36
  313.6 3.3 %copy.31 = bf16[2,1,256,2048]{3,2,1,0:T(8,128)(2,1)} copy(bf16[2,1,256,2048]{3,2,1,0:T(8,128)(2,1)} %get-tuple-element.45) | data formatting | bytes 4194304
  316.9 1.3 copy.32
  318.2 1.3 copy.33
  319.5 0.6 copy-done.3
  320.2 1.0 copy.34
  321.2 0.6 copy-done.9
  321.8 1.0 copy.35
  322.8 1.0 copy.36
  (37 shorter events, 0.1 us)
Async XLA Ops:
  7.2 3.0 copy-start.14
  7.2 3.0 copy-start.13
  7.2 146.8 %all-gather.4.cloned.1.call-start = ((), (), s32[]{:S(2)}) async-start(), calls=%async_computation.1 | async-start | bytes 7520256 | tf_op jit(solution)/shard_map/all_gather | solution.py:320
  8.6 3.0 copy-start.15
  8.6 3.0 copy-start.8
  11.5 200.4 %all-gather.6.cloned.1.call-start = ((), (), s32[]{:S(2)}) async-start(), calls=%async_computation.3 | async-start | bytes 4718592 | tf_op jit(solution)/shard_map/all_gather | solution.py:354
  15.1 68.4 %copy-start.4 = (f32[1,8,64,1024]{3,2,1,0:T(8,128)S(1)}, f32[1,8,64,1024]{3,2,1,0:T(8,128)}, u32[]{:S(2)}) copy-start(f32[1,8,64,1024]{3,2,1,0:T(8,128)} %param.16) | copy-start | bytes 6291460
  84.7 71.5 %copy-start.7 = (bf16[2,1,256,2048]{3,2,1,0:T(8,128)(2,1)S(1)}, bf16[2,1,256,2048]{3,2,1,0:T(8,128)(2,1)}, u32[]{:S(2)}) copy-start(bf16[2,1,256,2048]{3,2,1,0:T(8,128)(2,1)} %get-tuple-element.45) | copy-start | bytes 6291460
  155.2 6.0 %slice-start = ((s8[6684672]{0:T(1024)(128)(4,1)}), s8[4194304]{0:T(1024)(128)(4,1)S(1)}, s32[]{:S(2)}) async-start(s8[6684672]{0:T(1024)(128)(4,1)} %bitcast.66), calls=%async_computation.4 | async-start | bytes 8388608
  156.2 5.0 %slice-start.1 = ((s8[6684672]{0:T(1024)(128)(4,1)}), s8[2490368]{0:T(1024)(128)(4,1)S(1)}, s32[]{:S(2)}) async-start(s8[6684672]{0:T(1024)(128)(4,1)} %bitcast.66), calls=%async_computation.5 | async-start | bytes 4980736
  161.2 1.9 copy-start.5
  167.3 1.7 copy-start.10
  167.4 2.3 copy-start.11
  167.4 2.3 copy-start.12
  168.7 142.5 %reduce-scatter.2.cloned.1.call-start = ((), (), s32[]{:S(2)}) async-start(), calls=%async_computation.2 | async-start | bytes 3538944 | tf_op jit(solution)/shard_map/reduce_scatter | solution.py:362
  211.9 2.4 copy-start
  211.9 2.9 copy-start.1
  313.6 3.3 %copy-start.6 = (bf16[2,1,256,2048]{3,2,1,0:T(8,128)(2,1)S(1)}, bf16[2,1,256,2048]{3,2,1,0:T(8,128)(2,1)}, u32[]{:S(2)}) copy-start(bf16[2,1,256,2048]{3,2,1,0:T(8,128)(2,1)} %get-tuple-element.46) | copy-start | bytes 6291460
  318.2 2.0 copy-start.3
  320.2 1.6 copy-start.9
  320.2 2.6 copy-start.2
Sparse Core Ops, SparseCore 0:
  11.7 142.2 all-gather.3
  168.8 43.0 all-gather.5
  219.6 91.4 reduce-scatter.1

commit v3 on v2

--- a/solution.py
+++ b/solution.py
@@ -38,13 +38,12 @@
     )
 
 
-def wide_kernel(dims, g_loc, u_loc, g_out, u_out, send, recv, own, f_send, f_recv):
+def wide_steps(dims, g_loc, u_loc, g_out, u_out, send, recv, own, f_send, f_recv):
     n_gr, n_fs, n_tp = dims
     gr, fs, tp = lax.axis_index("gr"), lax.axis_index("fs"), lax.axis_index("tp")
     held = g_loc.shape[0] // n_fs
     rows, cols = g_loc.shape[1], g_loc.shape[2]
     per = g_out.shape[2] // rows
-    greet_group(dims, gr, fs, tp, pltpu.get_barrier_semaphore())
     to_tp = fs // per
 
     def place(out):
@@ -77,6 +76,7 @@
         @pl.when(to_tp != tp)
         def _():
             wide(loc, out, m, 0).start()
+        yield
     for loc, out, m in pairs:
         for j in range(per):
             for t in range(n_tp):
@@ -92,6 +92,7 @@
                     forward(n_gr, part, recv.at[m, j, t], recv.at[m, j, t], 1).wait_recv()
                 for p in range(1, n_gr):
                     forward(n_gr, part, f_send.at[m, j, t, p - 1], f_recv.at[m, j, t, p - 1], p).start()
+        yield
     for loc, out, m in pairs:
         for d in range(1, n_fs):
             wide(loc, out, m, d).wait_send()
@@ -107,12 +108,11 @@
                     forward(n_gr, block(out, (gr + n_gr - p) % n_gr, j, t), *sems, p).wait_recv()
 
 
-def tall_kernel(dims, d_loc, d_out, send, recv, own, f_send, f_recv):
+def tall_steps(dims, d_loc, d_out, send, recv, own, f_send, f_recv):
     n_gr, n_fs, n_tp = dims
     gr, fs, tp = lax.axis_index("gr"), lax.axis_index("fs"), lax.axis_index("tp")
     held = d_loc.shape[0] // n_fs
     rows = d_loc.shape[1]
-    greet_group(dims, gr, fs, tp, pltpu.get_barrier_semaphore())
 
     def block(g, s):
         start = s * rows if isinstance(s, int) else pl.multiple_of(s * rows, rows)
@@ -130,6 +130,7 @@
     for d in range(1, n_fs):
         tall(d).start()
     mine.start()
+    yield
     for s in range(n_fs):
         @pl.when(s == fs)
         def _():
@@ -140,6 +141,7 @@
             forward(n_gr, block(gr, s), recv.at[s], recv.at[s], 1).wait_recv()
         for p in range(1, n_gr):
             forward(n_gr, block(gr, s), f_send.at[s, p - 1], f_recv.at[s, p - 1], p).start()
+    yield
     for d in range(1, n_fs):
         tall(d).wait_send()
     for s in range(n_fs):
@@ -149,28 +151,19 @@
             forward(n_gr, block((gr + n_gr - p) % n_gr, s), *sems, p).wait_recv()
 
 
-def gather_kernel(dims, inner, number, *refs):
+def gather_steps(dims, inner, number, *refs):
     n_gr, n_fs, n_tp = dims
     gr, fs, tp = lax.axis_index("gr"), lax.axis_index("fs"), lax.axis_index("tp")
     ins, outs = refs[:number], refs[number:2 * number]
     z_send, z_recv, y_send, y_recv, own = refs[2 * number:]
     nz = n_fs // inner
     z, y = fs // inner, fs % inner
-    barrier = pltpu.get_barrier_semaphore()
 
     def when_next(way, act):
         pl.when(z < nz - 1 if way == 0 else z > 0)(act)
 
     def beside(way):
         return (gr, (z + 1 if way == 0 else z - 1) * inner + y, tp)
-
-    for q in range(1, inner):
-        pl.semaphore_signal(barrier, inc=1, device_id=(gr, z * inner + (y + q) % inner, tp), device_id_type=MESH)
-    for way in (0, 1):
-        when_next(way, lambda way=way: pl.semaphore_signal(
-            barrier, inc=1, device_id=beside(way), device_id_type=MESH))
-    peers = inner - 1 + (z > 0).astype(jnp.int32) + (z < nz - 1).astype(jnp.int32)
-    pl.semaphore_wait(barrier, peers)
 
     def block(m, zz, yy):
         rows = ins[m].shape[0]
@@ -219,6 +212,7 @@
             y_copy(m, q, 0, 0, y).start()
     for m in range(number):
         own_copy(m).start()
+    yield
     for d, way in places[1:]:
         def pass_on(d=d, way=way):
             for m in range(number):
@@ -228,6 +222,8 @@
                 for q in range(1, inner):
                     y_copy(m, q, way, d, y).start()
         steps(d, way, pass_on)
+        if way:
+            yield
     for m in range(number):
         for way in (0, 1):
             when_next(way, lambda m=m, way=way: z_copy(m, way, 0).wait_send())
@@ -244,9 +240,40 @@
         own_copy(m).wait()
 
 
-def call(body, outs, sems, ident, work, *args):
+def run_steps(first, second):
+    live = [first, second]
+    while live:
+        for steps in list(live):
+            if next(steps, live) is live:
+                live.remove(steps)
+
+
+def fused_kernel(dims, inner, number, main_steps, main_ins, main_outs, main_sems, *refs):
+    gr, fs, tp = lax.axis_index("gr"), lax.axis_index("fs"), lax.axis_index("tp")
+    greet_group(dims, gr, fs, tp, pltpu.get_barrier_semaphore())
+    edges = [0]
+    for n in (number, main_ins, number, main_outs, 5, main_sems):
+        edges.append(edges[-1] + n)
+    a, b, c, d, e, f = [refs[edges[i]:edges[i + 1]] for i in range(6)]
+    run_steps(gather_steps(dims, inner, number, *a, *c, *e), main_steps(dims, *b, *d, *f))
+
+
+def exchange(dims, ident, work, main_steps, arrays, main_args, main_outs, main_sems):
+    n_fs = dims[1]
+    inner = 2 if n_fs % 2 == 0 else 1
+    nz = n_fs // inner
+    number = len(arrays)
+    outs = tuple(jax.ShapeDtypeStruct((n_fs * a.shape[0], a.shape[1]), a.dtype) for a in arrays)
+    chain = (number, 2, max(1, nz - 1))
+    across = (number, max(1, inner - 1), 2 * nz - 1)
+    sems = [chain, chain, across, across, (number,), *main_sems]
+    args = (*arrays, *main_args)
+    outs = outs + tuple(main_outs)
     return pl.pallas_call(
-        body,
+        functools.partial(
+            fused_kernel, dims, inner, number, main_steps,
+            len(main_args), len(main_outs), len(main_sems),
+        ),
         out_shape=outs,
         in_specs=[pl.BlockSpec(memory_space=pl.ANY)] * len(args),
         out_specs=tuple(pl.BlockSpec(memory_space=pl.ANY) for _ in outs),
@@ -256,39 +283,25 @@
     )(*args)
 
 
-def exchange_wide(dims, g_loc, u_loc):
+def exchange_wide(dims, rows_here, g_loc, u_loc):
     n_gr, n_fs, n_tp = dims
     count, rows, cols = g_loc.shape
     per = n_fs // n_tp
     out = jax.ShapeDtypeStruct((n_gr, count // n_fs, per * rows, n_tp * cols), g_loc.dtype)
     halves = (2, per, n_tp, n_gr - 1)
-    return call(
-        functools.partial(wide_kernel, dims), (out, out),
-        [(2, n_fs), (2, per, n_tp), (2,), halves, halves], 1, 200 << 20, g_loc, u_loc,
-    )
-
-
-def exchange_tall(dims, d_loc):
+    return exchange(
+        dims, 1, 200 << 20, wide_steps, (rows_here,), (g_loc, u_loc), (out, out),
+        [(2, n_fs), (2, per, n_tp), (2,), halves, halves],
+    )
+
+
+def exchange_tall(dims, shared_here, d_loc):
     n_gr, n_fs, n_tp = dims
     count, rows, cols = d_loc.shape
     out = jax.ShapeDtypeStruct((n_gr, count // n_fs, n_fs * rows, cols), d_loc.dtype)
-    return call(
-        functools.partial(tall_kernel, dims), (out,),
-        [(n_fs,), (n_fs,), (), (n_fs, n_gr - 1), (n_fs, n_gr - 1)], 2, 100 << 20, d_loc,
-    )[0]
-
-
-def gather_fs(dims, ident, work, *arrays):
-    n_fs = dims[1]
-    inner = 2 if n_fs % 2 == 0 else 1
-    nz = n_fs // inner
-    number = len(arrays)
-    outs = tuple(jax.ShapeDtypeStruct((n_fs * a.shape[0], a.shape[1]), a.dtype) for a in arrays)
-    chain = (number, 2, max(1, nz - 1))
-    across = (number, max(1, inner - 1), 2 * nz - 1)
-    return call(
-        functools.partial(gather_kernel, dims, inner, number), outs,
-        [chain, chain, across, across, (number,)], ident, work, *arrays,
+    return exchange(
+        dims, 2, 100 << 20, tall_steps, shared_here, (d_loc,), (out,),
+        [(n_fs,), (n_fs,), (), (n_fs, n_gr - 1), (n_fs, n_gr - 1)],
     )
 
 
@@ -317,7 +330,7 @@
         [high.astype(bf), (weight - high).astype(bf), jnp.zeros((tok_count, extra - 2 * count), bf)],
         axis=1,
     )
-    rows_all = lax.all_gather(jnp.concatenate([normed, tail], axis=1), "fs", axis=0, tiled=True)
+    rows_here = jnp.concatenate([normed, tail], axis=1)
 
     gain_shared = lax.dynamic_slice_in_dim(
         norm_gain, fs_index * gate_shared.shape[0], gate_shared.shape[0], 0
@@ -329,8 +342,9 @@
     )
 
     gain_cols = lax.dynamic_slice_in_dim(norm_gain, tp_index * cols, cols, 0)
-    gate_w, up_w = exchange_wide(
+    rows_all, gate_w, up_w = exchange_wide(
         dims,
+        rows_here,
         (gate_experts[0] * gain_cols[None, None, :]).astype(bf),
         (up_experts[0] * gain_cols[None, None, :]).astype(bf),
     )
@@ -349,16 +363,17 @@
             upper = lax.dot_general(x, up_w[g, k], (((1,), (1,)), ((), ())), preferred_element_type=f32)
             parts.append((jax.nn.silu(gate) * upper * w_here[:, k:k + 1]).astype(bf))
     hidden = jnp.stack(parts)
-    hidden, down_local = lax.optimization_barrier((hidden, down_experts[0].astype(bf)))
-    down_w = exchange_tall(dims, down_local)
+    hidden, down_local, shared_here = lax.optimization_barrier(
+        (hidden, down_experts[0].astype(bf), shared_here)
+    )
+    gate_sw, up_sw, down_sw, down_w = exchange_tall(dims, shared_here, down_local)
     hidden = lax.all_gather(hidden, "tp", axis=0, tiled=False)
     partial = jnp.zeros((), f32)
     down_flat = down_w.reshape(n_gr * held, n_tp, units, cols)
     for i in range(n_gr * held):
         for t in range(n_tp):
             partial = partial + jnp.dot(hidden[t, i], down_flat[i, t], preferred_element_type=f32)
-    partial, shared_here = lax.optimization_barrier((partial.astype(bf), shared_here))
-    gate_sw, up_sw, down_sw = gather_fs(dims, 3, 60 << 20, *shared_here)
+    partial, normed = lax.optimization_barrier((partial.astype(bf), normed))
     routed = lax.psum_scatter(partial, "fs", scatter_dimension=0, tiled=True)
 
     shared_hidden = (

time: 331 us -> 316 us (0.955)
  waiting for transfers between devices: 107 us -> 63.5 us
  Pallas kernels: 156 us -> 176 us
  matrix products: 23.8 us -> 29.6 us
    all_gather x1 -> x0, waiting for transfers between devices: 69.3 us -> none  [on_device(): lax.all_gather(jnp.concatenate([normed, tail], axis=1), 'fs', axis=0, til...]
    reduce_scatter x1, waiting for transfers between devices: 17.6 us -> 63.4 us  [on_device(): routed = lax.psum_scatter(partial, 'fs', scatter_dimension=0, tiled=True)]
    pallas_call x3 -> x2, Pallas kernels: 156 us -> 176 us  [exchange(): pl.pallas_call(functools.partial(fused_kernel, dims, inner, number, main_...]
    all_gather x1, waiting for transfers between devices: 19.8 us -> 0.02 us  [on_device(): hidden = lax.all_gather(hidden, 'tp', axis=0, tiled=False)]
    dot_general x2, matrix products: 4.17 us -> 7.6 us  [on_device(): lax.dot_general(x, up_w[g, k], (((1,), (1,)), ((), ())), preferred_elemen...]
    unnamed x42 -> x44, local copies, waits for them, and re-layouts: 10.7 us -> 10.7 us
  transfers between devices with their start and end apart: 3 -> 2, of which waited for: 3 -> 1; matrix products, arithmetic and copies ran while one was open for 3% -> 1% of each run, Pallas kernels for 47% -> 17%
where the time goes in v3:
time: 316 us
  Pallas kernels  176 us (56%)
  waiting for transfers between devices  63.5 us (20%)
  matrix products  29.6 us (9%)
  between operations  14.3 us (5%)
  other arithmetic  14.1 us (4%)
  local copies, waits for them, and re-layouts  13.1 us (4%)
  blocking collectives  5.29 us (2%)
    pallas_call x2, Pallas kernels, exchange(): pl.pallas_call(functools.partial(fused_kernel, dims, inner, number, main_...  176 us
    reduce_scatter x1, waiting for transfers between devices, on_device(): routed = lax.psum_scatter(partial, 'fs', scatter_dimension=0, tiled=True)  63.4 us
    unnamed x44, local copies, waits for them, and re-layouts  10.7 us
    dot_general x2, matrix products, on_device(): lax.dot_general(x, gate_w[g, k], (((1,), (1,)), ((), ())), preferred_elem...  9.16 us
    dot_general x2, matrix products, on_device(): lax.dot_general(x, up_w[g, k], (((1,), (1,)), ((), ())), preferred_elemen...  7.6 us
    dot_general x4, matrix products, on_device(): jnp.dot(hidden[t, i], down_flat[i, t], preferred_element_type=f32)  7.16 us
  transfers between devices with their start and end apart: 2, of which 1 were waited for; matrix products, arithmetic and copies ran while one was open for 1% of the time, Pallas kernels for 17%

profile of v3, /device:TPU:0, one launch (start us, length us, event | category | flops | bytes accessed | tf_op | source)
XLA Modules:
  0.0 315.8 jit_solution(10333539815235602071)
XLA Ops:
  7.2 0.0 all-gather.3.cloned.1.call-start
  7.2 0.9 select_reduce_fusion
  8.1 0.1 copy.25
  8.2 0.1 copy.26
  8.3 0.1 copy.27
  8.4 1.4 fusion.34
  9.8 1.3 fusion.35
  11.2 3.5 %fusion.32 = (bf16[8,64,1024]{2,1,0:T(8,128)(2,1)}, bf16[8,64,1024]{2,1,0:T(8,128)(2,1)}) fusion(f32[1,8,64,1024]{3,2,1,0:T(8,128)S(1)} %copy-done.7, f32[1024]{0:T(1024)S(1)} %dynamic_slice.12, f32[1,8,64,1024]{3,2,1,0:T(8,128)} %param.14), kind=kLoop, calls=%fused_computation.18 | loop fusion | flops 2097152 | bytes 6295552 | tf_op jit(solution)/shard_map/convert_element_type | solution.py:349
  14.7 1.1 concatenate.3.refs_0_
  15.8 122.3 %shard_map.153 = (bf16[1536,2176]{1,0:T(8,128)(2,1)}, bf16[2,1,256,2048]{3,2,1,0:T(8,128)(2,1)}, bf16[2,1,256,2048]{3,2,1,0:T(8,128)(2,1)}) custom-call(bf16[192,2176]{1,0:T(8,128)(2,1)} %concatenate.3.refs_0_, bf16[8,64,1024]{2,1,0:T(8,128)(2,1)} %get-tuple-element.40.refs_1_, bf16[8,64,1024]{2,1,0:T(8,128)(2,1)} %get-tuple-element.39.refs_2_), custom_call_target="tpu_custom_call" | custom-call | bytes 209715200 | tf_op jit(solution)/shard_map/pallas_call | solution.py:272
  138.1 1.4 convert_add_fusion
  139.5 6.2 %fusion.6 = f32[1536,256]{1,0:T(8,128)} fusion(bf16[1536,2176]{1,0:T(8,128)(2,1)} %get-tuple-element.21, bf16[2,1,256,2048]{3,2,1,0:T(8,128)(2,1)} %get-tuple-element.51), kind=kOutput, calls=%fused_computation.7 | convolution fusion | flops 1610612736 | bytes 8912896 | tf_op jit(solution)/shard_map/dot_general | solution.py:362
  145.7 3.0 fusion.2
  148.7 0.1 dynamic_slice.15
  148.8 2.8 convert_bitcast_fusion.refs_3_
  151.6 0.7 convert_element_type.71.refs_2_
  152.3 0.9 dynamic-slice_reduce_fusion.1
  153.2 0.0 slice-start.3
  153.2 0.0 copy-start.13
  153.3 5.5 %fusion.26 = bf16[1,1536,256]{2,1,0:T(8,128)(2,1)S(1)} fusion(bf16[1536,2176]{1,0:T(8,128)(2,1)} %get-tuple-element.21, f32[1536,256]{1,0:T(8,128)S(1)} %copy-done.14, bf16[2,1,256,2048]{3,2,1,0:T(8,128)(2,1)} %get-tuple-element.52, f32[1536]{0:T(1024)S(1)} %get-tuple-element.35), kind=kOutput, calls=%fused_computation.15 | convolution fusion | flops 1613365248 | bytes 9705472 | tf_op jit(solution)/shard_map/dot_general | solution.py:363
  158.8 2.1 fusion.29
  160.9 0.0 copy-start.10
  160.9 0.0 copy-start.11
  160.9 1.3 pad_maximum_fusion
  162.2 0.8 multiply_convert_fusion
  163.0 0.0 all-gather.3.cloned.1.call-update
  163.1 0.0 reduce-scatter.2.cloned.1.call-start
  163.1 53.6 %shard_map.154 = (bf16[2048,256]{1,0:T(8,128)(2,1)}, bf16[2048,256]{1,0:T(8,128)(2,1)}, bf16[512,1024]{1,0:T(8,128)(2,1)}, bf16[2,1,512,1024]{3,2,1,0:T(8,128)(2,1)}) custom-call(bf16[256,256]{1,0:T(8,128)(2,1)} %get-tuple-element.25.refs_0_, bf16[256,256]{1,0:T(8,128)(2,1)} %get-tuple-element.26.refs_1_, bf16[64,1024]{1,0:T(8,128)(2,1)} %convert_element_type.71.refs_2_, ...), custom_call_target="tpu_custom_call" | custom-call | bytes 104857600 | tf_op jit(solution)/shard_map/pallas_call | solution.py:272
  216.7 0.0 all-gather.3.cloned.1.call-done
  216.8 2.4 fusion.47
  219.2 0.5 copy-done.1
  219.7 1.0 fusion.48
  220.6 1.0 fusion.46
  221.6 2.8 add_convert_fusion
  224.4 0.0 reduce-scatter.2.cloned.1.call-update
  224.4 1.6 fusion.50
  226.0 1.6 fusion.37
  227.6 5.3 %all_gather.11 = bf16[192,512]{1,0:T(8,128)(2,1)S(1)} all-gather(bf16[192,256]{1,0:T(8,128)(2,1)S(1)} %fusion.37), channel_id=1, replica_groups=mesh['gr'=2,'fs'=8,'tp'=2] {'tp'}, dimensions={1}, use_global_device_ids=true | all-gather | bytes 294912 | tf_op jit(solution)/shard_map/all_gather | solution.py:383
  232.9 63.4 %reduce-scatter.2.cloned.1.call-done = bf16[192,1024]{1,0:T(8,128)(2,1)} async-done(((bf16[1536,1024]{1,0:T(8,128)(2,1)}), bf16[192,1024]{1,0:T(8,128)(2,1)}) %reduce-scatter.2.cloned.1.call-update) | async-done | bytes 393232 | tf_op jit(solution)/shard_map/reduce_scatter | solution.py:377
  296.4 2.4 fusion.36
  298.8 3.3 %copy.34 = bf16[2,1,256,2048]{3,2,1,0:T(8,128)(2,1)} copy(bf16[2,1,256,2048]{3,2,1,0:T(8,128)(2,1)} %get-tuple-element.51) | data formatting | bytes 4194304
  302.1 1.3 copy.35
  303.5 1.3 copy.36
  304.8 0.6 copy-done.3
  305.4 1.0 copy.37
  306.4 0.6 copy-done.8
  307.0 1.0 copy.38
  308.0 1.0 copy.39
  (38 shorter events, 0.1 us)
Async XLA Ops:
  7.2 4.0 %copy-start.12 = (f32[2048]{0:T(1024)S(1)}, f32[2048]{0:T(1024)}, u32[]{:S(2)}) copy-start(f32[2048]{0:T(1024)} %param.13) | copy-start | bytes 24580
  7.2 4.0 %copy-start.7 = (f32[1,8,64,1024]{3,2,1,0:T(8,128)S(1)}, f32[1,8,64,1024]{3,2,1,0:T(8,128)}, u32[]{:S(2)}) copy-start(f32[1,8,64,1024]{3,2,1,0:T(8,128)} %param.15) | copy-start | bytes 6291460
  7.2 209.5 %all-gather.3.cloned.1.call-start = ((), (), s32[]{:S(2)}) async-start(), calls=%async_computation.2 | async-start | bytes 4718592 | tf_op jit(solution)/shard_map/all_gather | solution.py:370
  138.1 7.7 %slice-start = ((s8[6684672]{0:T(1024)(128)(4,1)}), s8[4194304]{0:T(1024)(128)(4,1)S(1)}, s32[]{:S(2)}) async-start(s8[6684672]{0:T(1024)(128)(4,1)} %bitcast.66), calls=%async_computation.3 | async-start | bytes 8388608
  139.5 6.2 %copy-start.6 = (bf16[2,1,256,2048]{3,2,1,0:T(8,128)(2,1)S(1)}, bf16[2,1,256,2048]{3,2,1,0:T(8,128)(2,1)}, u32[]{:S(2)}) copy-start(bf16[2,1,256,2048]{3,2,1,0:T(8,128)(2,1)} %get-tuple-element.51) | copy-start | bytes 6291460
  139.5 6.2 %slice-start.1 = ((s8[6684672]{0:T(1024)(128)(4,1)}), s8[2490368]{0:T(1024)(128)(4,1)S(1)}, s32[]{:S(2)}) async-start(s8[6684672]{0:T(1024)(128)(4,1)} %bitcast.66), calls=%async_computation.4 | async-start | bytes 4980736
  148.7 2.9 copy-start.9
  148.8 4.4 %copy-start.14 = (f32[1536,256]{1,0:T(8,128)S(1)}, f32[1536,256]{1,0:T(8,128)}, u32[]{:S(2)}) copy-start(f32[1536,256]{1,0:T(8,128)} %fusion.6) | copy-start | bytes 4718596
  152.3 6.5 %slice-start.2 = ((s8[6684672]{0:T(1024)(128)(4,1)}), s8[4194304]{0:T(1024)(128)(4,1)S(1)}, s32[]{:S(2)}) async-start(s8[6684672]{0:T(1024)(128)(4,1)} %bitcast.68), calls=%async_computation.5 | async-start | bytes 8388608
  153.2 5.6 %copy-start.4 = (bf16[2,1,256,2048]{3,2,1,0:T(8,128)(2,1)S(1)}, bf16[2,1,256,2048]{3,2,1,0:T(8,128)(2,1)}, u32[]{:S(2)}) copy-start(bf16[2,1,256,2048]{3,2,1,0:T(8,128)(2,1)} %get-tuple-element.52) | copy-start | bytes 6291460
  153.2 5.6 %slice-start.3 = ((s8[6684672]{0:T(1024)(128)(4,1)}), s8[2490368]{0:T(1024)(128)(4,1)S(1)}, s32[]{:S(2)}) async-start(s8[6684672]{0:T(1024)(128)(4,1)} %bitcast.68), calls=%async_computation.6 | async-start | bytes 4980736
  153.2 5.6 %copy-start.13 = (f32[1536,256]{1,0:T(8,128)S(1)}, f32[1536,256]{1,0:T(8,128)}, u32[]{:S(2)}) copy-start(f32[1536,256]{1,0:T(8,128)} %fusion.2) | copy-start | bytes 4718596
  160.9 1.3 copy-start.10
  160.9 1.3 copy-start.11
  163.1 133.3 %reduce-scatter.2.cloned.1.call-start = ((), (), s32[]{:S(2)}) async-start(), calls=%async_computation.1 | async-start | bytes 3538944 | tf_op jit(solution)/shard_map/reduce_scatter | solution.py:377
  216.7 2.4 copy-start
  216.8 2.9 copy-start.1
  298.8 3.3 %copy-start.5 = (bf16[2,1,256,2048]{3,2,1,0:T(8,128)(2,1)S(1)}, bf16[2,1,256,2048]{3,2,1,0:T(8,128)(2,1)}, u32[]{:S(2)}) copy-start(bf16[2,1,256,2048]{3,2,1,0:T(8,128)(2,1)} %get-tuple-element.52) | copy-start | bytes 6291460
  303.5 2.0 copy-start.3
  305.4 1.6 copy-start.8
  305.4 2.6 copy-start.2
Sparse Core Ops, SparseCore 0:
  163.2 42.0 all-gather.2
  224.6 71.7 reduce-scatter.1

commit v4 on v3

--- a/solution.py
+++ b/solution.py
@@ -151,11 +151,11 @@
             forward(n_gr, block((gr + n_gr - p) % n_gr, s), *sems, p).wait_recv()
 
 
-def gather_steps(dims, inner, number, *refs):
+def gather_steps(dims, inner, number, parts, *refs):
     n_gr, n_fs, n_tp = dims
     gr, fs, tp = lax.axis_index("gr"), lax.axis_index("fs"), lax.axis_index("tp")
     ins, outs = refs[:number], refs[number:2 * number]
-    z_send, z_recv, y_send, y_recv, own = refs[2 * number:]
+    z_send, z_recv, y_send, y_recv, x_send, x_recv, own = refs[2 * number:]
     nz = n_fs // inner
     z, y = fs // inner, fs % inner
 
@@ -186,14 +186,46 @@
             recv_sem=z_recv.at[m, way, d - 1], device_id=beside(way), device_id_type=MESH,
         ).wait_recv()
 
+    def share(m, zz, yy, t):
+        rows = ins[m].shape[0]
+        sub = rows // parts
+        start = (zz * inner + yy) * rows + (t * sub if parts > 1 else 0)
+        return outs[m].at[pl.ds(pl.multiple_of(start, sub), sub), :]
+
+    def first_share(m):
+        sub = ins[m].shape[0] // parts
+        return ins[m].at[pl.ds(pl.multiple_of(tp * sub, sub), sub), :] if parts > 1 else ins[m]
+
     def y_copy(m, q, way, d, source):
-        part = block(m, at(way, d), source)
+        part = share(m, at(way, d), source, tp)
         i = d + way * (nz - 1) if d else 0
         return pltpu.make_async_remote_copy(
-            src_ref=ins[m] if d == 0 else part, dst_ref=part,
+            src_ref=first_share(m) if d == 0 else part, dst_ref=part,
             send_sem=y_send.at[m, q - 1, i], recv_sem=y_recv.at[m, q - 1, i],
             device_id=(gr, z * inner + (y + q) % inner, tp), device_id_type=MESH,
         )
+
+    def x_copy(m, q, way, d, r, holder):
+        part = share(m, at(way, d), (y + inner - q) % inner, holder)
+        i = d + way * (nz - 1) if d else 0
+        return pltpu.make_async_remote_copy(
+            src_ref=part, dst_ref=part,
+            send_sem=x_send.at[m, q - 1, i, r - 1], recv_sem=x_recv.at[m, q - 1, i, r - 1],
+            device_id=(gr, fs, (tp + r) % n_tp), device_id_type=MESH,
+        )
+
+    def hand_over(distance):
+        for d, way in places:
+            if d != distance:
+                continue
+
+            def act(d=d, way=way):
+                for m in range(number):
+                    for q in range(1, inner):
+                        y_copy(m, q, way, d, (y + inner - q) % inner).wait_recv()
+                        for r in range(1, parts):
+                            x_copy(m, q, way, d, r, tp).start()
+            steps(d, way, act)
 
     def own_copy(m):
         return pltpu.make_async_copy(ins[m], block(m, z, y), own.at[m])
@@ -223,7 +255,9 @@
                     y_copy(m, q, way, d, y).start()
         steps(d, way, pass_on)
         if way:
+            hand_over(d - 1)
             yield
+    hand_over(nz - 1)
     for m in range(number):
         for way in (0, 1):
             when_next(way, lambda m=m, way=way: z_copy(m, way, 0).wait_send())
@@ -234,7 +268,9 @@
                     when_next(way, lambda: z_copy(m, way, d).wait_send())
                 for q in range(1, inner):
                     y_copy(m, q, way, d, y).wait_send()
-                    y_copy(m, q, way, d, (y + inner - q) % inner).wait_recv()
+                    for r in range(1, parts):
+                        x_copy(m, q, way, d, r, tp).wait_send()
+                        x_copy(m, q, way, d, r, (tp + n_tp - r) % n_tp).wait_recv()
         steps(d, way, finish)
     for m in range(number):
         own_copy(m).wait()
@@ -248,17 +284,17 @@
                 live.remove(steps)
 
 
-def fused_kernel(dims, inner, number, main_steps, main_ins, main_outs, main_sems, *refs):
+def fused_kernel(dims, inner, number, parts, main_steps, main_ins, main_outs, main_sems, *refs):
     gr, fs, tp = lax.axis_index("gr"), lax.axis_index("fs"), lax.axis_index("tp")
     greet_group(dims, gr, fs, tp, pltpu.get_barrier_semaphore())
     edges = [0]
-    for n in (number, main_ins, number, main_outs, 5, main_sems):
+    for n in (number, main_ins, number, main_outs, 7, main_sems):
         edges.append(edges[-1] + n)
     a, b, c, d, e, f = [refs[edges[i]:edges[i + 1]] for i in range(6)]
-    run_steps(gather_steps(dims, inner, number, *a, *c, *e), main_steps(dims, *b, *d, *f))
-
-
-def exchange(dims, ident, work, main_steps, arrays, main_args, main_outs, main_sems):
+    run_steps(gather_steps(dims, inner, number, parts, *a, *c, *e), main_steps(dims, *b, *d, *f))
+
+
+def exchange(dims, ident, work, main_steps, same_on_tp, arrays, main_args, main_outs, main_sems):
     n_fs = dims[1]
     inner = 2 if n_fs % 2 == 0 else 1
     nz = n_fs // inner
@@ -266,12 +302,15 @@
     outs = tuple(jax.ShapeDtypeStruct((n_fs * a.shape[0], a.shape[1]), a.dtype) for a in arrays)
     chain = (number, 2, max(1, nz - 1))
     across = (number, max(1, inner - 1), 2 * nz - 1)
-    sems = [chain, chain, across, across, (number,), *main_sems]
+    n_tp = dims[2]
+    parts = n_tp if same_on_tp and all(a.shape[0] % (8 * n_tp) == 0 for a in arrays) else 1
+    over = (*across, max(1, parts - 1))
+    sems = [chain, chain, across, across, over, over, (number,), *main_sems]
     args = (*arrays, *main_args)
     outs = outs + tuple(main_outs)
     return pl.pallas_call(
         functools.partial(
-            fused_kernel, dims, inner, number, main_steps,
+            fused_kernel, dims, inner, number, parts, main_steps,
             len(main_args), len(main_outs), len(main_sems),
         ),
         out_shape=outs,
@@ -290,7 +329,7 @@
     out = jax.ShapeDtypeStruct((n_gr, count // n_fs, per * rows, n_tp * cols), g_loc.dtype)
     halves = (2, per, n_tp, n_gr - 1)
     return exchange(
-        dims, 1, 200 << 20, wide_steps, (rows_here,), (g_loc, u_loc), (out, out),
+        dims, 1, 200 << 20, wide_steps, True, (rows_here,), (g_loc, u_loc), (out, out),
         [(2, n_fs), (2, per, n_tp), (2,), halves, halves],
     )
 
@@ -300,7 +339,7 @@
     count, rows, cols = d_loc.shape
     out = jax.ShapeDtypeStruct((n_gr, count // n_fs, n_fs * rows, cols), d_loc.dtype)
     return exchange(
-        dims, 2, 100 << 20, tall_steps, shared_here, (d_loc,), (out,),
+        dims, 2, 100 << 20, tall_steps, False, shared_here, (d_loc,), (out,),
         [(n_fs,), (n_fs,), (), (n_fs, n_gr - 1), (n_fs, n_gr - 1)],
     )
 

time: 316 us -> 319 us (level)
  no operation moved by 1% of the time
where the time goes in v4:
time: 319 us
  Pallas kernels  178 us (56%)
  waiting for transfers between devices  64.1 us (20%)
  matrix products  29.6 us (9%)
  between operations  14.3 us (4%)
  other arithmetic  14.1 us (4%)
  local copies, waits for them, and re-layouts  13.1 us (4%)
  blocking collectives  5.29 us (2%)
    pallas_call x2, Pallas kernels, exchange(): pl.pallas_call(functools.partial(fused_kernel, dims, inner, number, parts...  178 us
    reduce_scatter x1, waiting for transfers between devices, on_device(): routed = lax.psum_scatter(partial, 'fs', scatter_dimension=0, tiled=True)  64.1 us
    unnamed x44, local copies, waits for them, and re-layouts  10.7 us
    dot_general x2, matrix products, on_device(): lax.dot_general(x, gate_w[g, k], (((1,), (1,)), ((), ())), preferred_elem...  9.16 us
    dot_general x2, matrix products, on_device(): lax.dot_general(x, up_w[g, k], (((1,), (1,)), ((), ())), preferred_elemen...  7.6 us
    dot_general x4, matrix products, on_device(): jnp.dot(hidden[t, i], down_flat[i, t], preferred_element_type=f32)  7.16 us
  transfers between devices with their start and end apart: 2, of which 1 were waited for; matrix products, arithmetic and copies ran while one was open for 1% of the time, Pallas kernels for 17%

profile of v4, /device:TPU:0, one launch (start us, length us, event | category | flops | bytes accessed | tf_op | source)
XLA Modules:
  0.0 319.1 jit_solution(13502029734633014993)
XLA Ops:
  7.2 0.0 all-gather.3.cloned.1.call-start
  7.2 0.9 select_reduce_fusion
  8.1 0.1 copy.25
  8.2 0.1 copy.26
  8.3 0.1 copy.27
  8.4 1.4 fusion.34
  9.8 1.3 fusion.35
  11.2 3.5 %fusion.32 = (bf16[8,64,1024]{2,1,0:T(8,128)(2,1)}, bf16[8,64,1024]{2,1,0:T(8,128)(2,1)}) fusion(f32[1,8,64,1024]{3,2,1,0:T(8,128)S(1)} %copy-done.7, f32[1024]{0:T(1024)S(1)} %dynamic_slice.12, f32[1,8,64,1024]{3,2,1,0:T(8,128)} %param.14), kind=kLoop, calls=%fused_computation.18 | loop fusion | flops 2097152 | bytes 6295552 | tf_op jit(solution)/shard_map/convert_element_type | solution.py:388
  14.7 1.1 concatenate.3.refs_0_
  15.8 124.5 %shard_map.153 = (bf16[1536,2176]{1,0:T(8,128)(2,1)}, bf16[2,1,256,2048]{3,2,1,0:T(8,128)(2,1)}, bf16[2,1,256,2048]{3,2,1,0:T(8,128)(2,1)}) custom-call(bf16[192,2176]{1,0:T(8,128)(2,1)} %concatenate.3.refs_0_, bf16[8,64,1024]{2,1,0:T(8,128)(2,1)} %get-tuple-element.40.refs_1_, bf16[8,64,1024]{2,1,0:T(8,128)(2,1)} %get-tuple-element.39.refs_2_), custom_call_target="tpu_custom_call" | custom-call | bytes 209715200 | tf_op jit(solution)/shard_map/pallas_call | solution.py:311
  140.3 1.4 convert_add_fusion
  141.8 0.0 slice-start.1
  141.8 6.2 %fusion.6 = f32[1536,256]{1,0:T(8,128)} fusion(bf16[1536,2176]{1,0:T(8,128)(2,1)} %get-tuple-element.21, bf16[2,1,256,2048]{3,2,1,0:T(8,128)(2,1)} %get-tuple-element.51), kind=kOutput, calls=%fused_computation.7 | convolution fusion | flops 1610612736 | bytes 8912896 | tf_op jit(solution)/shard_map/dot_general | solution.py:401
  148.0 3.0 fusion.2
  151.0 0.1 dynamic_slice.15
  151.0 2.8 convert_bitcast_fusion.refs_3_
  153.9 0.7 convert_element_type.71.refs_2_
  154.6 0.9 dynamic-slice_reduce_fusion.1
  155.5 0.0 copy-start.13
  155.5 5.5 %fusion.26 = bf16[1,1536,256]{2,1,0:T(8,128)(2,1)S(1)} fusion(bf16[1536,2176]{1,0:T(8,128)(2,1)} %get-tuple-element.21, f32[1536,256]{1,0:T(8,128)S(1)} %copy-done.14, bf16[2,1,256,2048]{3,2,1,0:T(8,128)(2,1)} %get-tuple-element.52, f32[1536]{0:T(1024)S(1)} %get-tuple-element.35), kind=kOutput, calls=%fused_computation.15 | convolution fusion | flops 1613365248 | bytes 9705472 | tf_op jit(solution)/shard_map/dot_general | solution.py:402
  161.1 2.1 fusion.29
  163.2 0.0 copy-start.10
  163.2 0.0 copy-start.11
  163.2 1.3 pad_maximum_fusion
  164.5 0.8 multiply_convert_fusion
  165.3 0.0 all-gather.3.cloned.1.call-update
  165.3 0.0 reduce-scatter.2.cloned.1.call-start
  165.4 54.0 %shard_map.154 = (bf16[2048,256]{1,0:T(8,128)(2,1)}, bf16[2048,256]{1,0:T(8,128)(2,1)}, bf16[512,1024]{1,0:T(8,128)(2,1)}, bf16[2,1,512,1024]{3,2,1,0:T(8,128)(2,1)}) custom-call(bf16[256,256]{1,0:T(8,128)(2,1)} %get-tuple-element.25.refs_0_, bf16[256,256]{1,0:T(8,128)(2,1)} %get-tuple-element.26.refs_1_, bf16[64,1024]{1,0:T(8,128)(2,1)} %convert_element_type.71.refs_2_, ...), custom_call_target="tpu_custom_call" | custom-call | bytes 104857600 | tf_op jit(solution)/shard_map/pallas_call | solution.py:311
  219.3 0.0 all-gather.3.cloned.1.call-done
  219.4 2.4 fusion.47
  221.8 0.5 copy-done.1
  222.3 1.0 fusion.48
  223.3 1.0 fusion.46
  224.2 2.8 add_convert_fusion
  227.0 0.0 reduce-scatter.2.cloned.1.call-update
  227.0 1.6 fusion.50
  228.7 1.6 fusion.37
  230.3 5.3 %all_gather.11 = bf16[192,512]{1,0:T(8,128)(2,1)S(1)} all-gather(bf16[192,256]{1,0:T(8,128)(2,1)S(1)} %fusion.37), channel_id=1, replica_groups=mesh['gr'=2,'fs'=8,'tp'=2] {'tp'}, dimensions={1}, use_global_device_ids=true | all-gather | bytes 294912 | tf_op jit(solution)/shard_map/all_gather | solution.py:422
  235.5 64.1 %reduce-scatter.2.cloned.1.call-done = bf16[192,1024]{1,0:T(8,128)(2,1)} async-done(((bf16[1536,1024]{1,0:T(8,128)(2,1)}), bf16[192,1024]{1,0:T(8,128)(2,1)}) %reduce-scatter.2.cloned.1.call-update) | async-done | bytes 393232 | tf_op jit(solution)/shard_map/reduce_scatter | solution.py:416
  299.6 2.4 fusion.36
  302.1 3.3 %copy.34 = bf16[2,1,256,2048]{3,2,1,0:T(8,128)(2,1)} copy(bf16[2,1,256,2048]{3,2,1,0:T(8,128)(2,1)} %get-tuple-element.51) | data formatting | bytes 4194304
  305.4 1.3 copy.35
  306.7 1.3 copy.36
  308.0 0.6 copy-done.3
  308.7 1.0 copy.37
  309.6 0.6 copy-done.8
  310.3 1.0 copy.38
  311.2 1.0 copy.39
  (38 shorter events, 0.1 us)
Async XLA Ops:
  7.2 4.0 %copy-start.12 = (f32[2048]{0:T(1024)S(1)}, f32[2048]{0:T(1024)}, u32[]{:S(2)}) copy-start(f32[2048]{0:T(1024)} %param.13) | copy-start | bytes 24580
  7.2 4.0 %copy-start.7 = (f32[1,8,64,1024]{3,2,1,0:T(8,128)S(1)}, f32[1,8,64,1024]{3,2,1,0:T(8,128)}, u32[]{:S(2)}) copy-start(f32[1,8,64,1024]{3,2,1,0:T(8,128)} %param.15) | copy-start | bytes 6291460
  7.2 212.2 %all-gather.3.cloned.1.call-start = ((), (), s32[]{:S(2)}) async-start(), calls=%async_computation.2 | async-start | bytes 4718592 | tf_op jit(solution)/shard_map/all_gather | solution.py:409
  140.3 7.7 %slice-start = ((s8[6684672]{0:T(1024)(128)(4,1)}), s8[4194304]{0:T(1024)(128)(4,1)S(1)}, s32[]{:S(2)}) async-start(s8[6684672]{0:T(1024)(128)(4,1)} %bitcast.66), calls=%async_computation.3 | async-start | bytes 8388608
  141.8 6.2 %copy-start.6 = (bf16[2,1,256,2048]{3,2,1,0:T(8,128)(2,1)S(1)}, bf16[2,1,256,2048]{3,2,1,0:T(8,128)(2,1)}, u32[]{:S(2)}) copy-start(bf16[2,1,256,2048]{3,2,1,0:T(8,128)(2,1)} %get-tuple-element.51) | copy-start | bytes 6291460
  141.8 6.2 %slice-start.1 = ((s8[6684672]{0:T(1024)(128)(4,1)}), s8[2490368]{0:T(1024)(128)(4,1)S(1)}, s32[]{:S(2)}) async-start(s8[6684672]{0:T(1024)(128)(4,1)} %bitcast.66), calls=%async_computation.4 | async-start | bytes 4980736
  151.0 2.9 copy-start.9
  151.0 4.4 %copy-start.14 = (f32[1536,256]{1,0:T(8,128)S(1)}, f32[1536,256]{1,0:T(8,128)}, u32[]{:S(2)}) copy-start(f32[1536,256]{1,0:T(8,128)} %fusion.6) | copy-start | bytes 4718596
  154.6 6.5 %slice-start.2 = ((s8[6684672]{0:T(1024)(128)(4,1)}), s8[4194304]{0:T(1024)(128)(4,1)S(1)}, s32[]{:S(2)}) async-start(s8[6684672]{0:T(1024)(128)(4,1)} %bitcast.68), calls=%async_computation.5 | async-start | bytes 8388608
  155.5 5.6 %copy-start.4 = (bf16[2,1,256,2048]{3,2,1,0:T(8,128)(2,1)S(1)}, bf16[2,1,256,2048]{3,2,1,0:T(8,128)(2,1)}, u32[]{:S(2)}) copy-start(bf16[2,1,256,2048]{3,2,1,0:T(8,128)(2,1)} %get-tuple-element.52) | copy-start | bytes 6291460
  155.5 5.6 %slice-start.3 = ((s8[6684672]{0:T(1024)(128)(4,1)}), s8[2490368]{0:T(1024)(128)(4,1)S(1)}, s32[]{:S(2)}) async-start(s8[6684672]{0:T(1024)(128)(4,1)} %bitcast.68), calls=%async_computation.6 | async-start | bytes 4980736
  155.5 5.6 %copy-start.13 = (f32[1536,256]{1,0:T(8,128)S(1)}, f32[1536,256]{1,0:T(8,128)}, u32[]{:S(2)}) copy-start(f32[1536,256]{1,0:T(8,128)} %fusion.2) | copy-start | bytes 4718596
  163.2 1.3 copy-start.10
  163.2 1.3 copy-start.11
  165.3 134.3 %reduce-scatter.2.cloned.1.call-start = ((), (), s32[]{:S(2)}) async-start(), calls=%async_computation.1 | async-start | bytes 3538944 | tf_op jit(solution)/shard_map/reduce_scatter | solution.py:416
  219.4 2.4 copy-start
  219.4 2.9 copy-start.1
  302.1 3.3 %copy-start.5 = (bf16[2,1,256,2048]{3,2,1,0:T(8,128)(2,1)S(1)}, bf16[2,1,256,2048]{3,2,1,0:T(8,128)(2,1)}, u32[]{:S(2)}) copy-start(bf16[2,1,256,2048]{3,2,1,0:T(8,128)(2,1)} %get-tuple-element.52) | copy-start | bytes 6291460
  306.7 2.0 copy-start.3
  308.7 1.6 copy-start.8
  308.7 2.6 copy-start.2
Sparse Core Ops, SparseCore 0:
  165.4 41.0 all-gather.2
  227.2 72.4 reduce-scatter.1
